TPU v7x, 128 devices: a whole 4x4x4 slice. The times are simulated.
128 devices in a mesh: sp: 32 (over z, y, core), tp: 4 (over x).
Axes of the slice: x: 4, y: 4, z: 4, core: 2. Of those that a mesh axis runs over, the one named last changes fastest.
Arguments:
- residual: bfloat16 [32768, 2048], P('sp', 'tp'), may hold values from -64 to 64
- rotated_query_rows: bfloat16 [32768, 1536], P('sp', 'tp'), may hold values from -256 to 256
- rotated_key_rows: bfloat16 [32768, 512], P('sp', 'tp'), may hold values from -6 to 6
- value_matrix_rows: bfloat16 [32768, 512], P('sp', 'tp'), may hold values from -16 to 16
- head_sink_logit: float32 [24], P('tp'), may hold values from 2 to 7
- out_proj: bfloat16 [1536, 2048], P('tp'), may hold values from -1.2247449 to 1.2247449
- gain_mix: float32 [2048], replicated, may hold values from 0.1 to 1.9
- gain_pre: float32 [2048], replicated, may hold values from 0.1 to 1.9
- gain_post: float32 [2048], replicated, may hold values from 0.1 to 1.9
- gate_proj: bfloat16 [2048, 5632], P('sp', 'tp'), may hold values from -0.125 to 0.125
- up_proj: bfloat16 [2048, 5632], P('sp', 'tp'), may hold values from -0.125 to 0.125
- down_proj: bfloat16 [5632, 2048], P('tp', 'sp'), may hold values from -0.21320072 to 0.21320072
Outputs:
- layer_out: bfloat16 [32768, 2048], P('sp', 'tp')
All inputs are finite; a program needn't handle non-finite values.
Results may differ from a plain program's by a relative error of at most 0.0095.
Values may be sent and summed in bfloat16 or wider, within the bound.
A program may use at most 128 MiB of HBM per device.

v0:
```python
import jax
import jax.numpy as jnp
from jax import lax
from jax.sharding import PartitionSpec as P

HEAD_WIDTH = 64
WINDOW = 128


norm_eps = 1e-06


def rows_first(arrays, axis, dims):
    turned = [jnp.moveaxis(a, dim, 0) for a, dim in zip(arrays, dims)]
    widths = [t[0].size for t in turned]
    both = jnp.concatenate([t.reshape(-1, w) for t, w in zip(turned, widths)], axis=1)
    out = lax.all_gather(both, axis, axis=0, tiled=True)
    tiles = jnp.split(out, [sum(widths[:k]) for k in range(1, len(widths))], axis=1)
    return tuple(
        (
            jnp.moveaxis(b.reshape(-1, *t.shape[1:]), 0, dim)
            for b, t, dim in zip(tiles, turned, dims)
        )
    )


def with_halo(shard, sides, width):
    for axis, dim in sides:
        count, length = (lax.axis_size(axis), shard.shape[dim])
        up = [(i, (i + 1) % count) for i in range(count - 1)]
        down = [(j, i) for i, j in up]
        last = lax.slice_in_dim(shard, length - width, length, axis=dim)
        first = lax.slice_in_dim(shard, 0, width, axis=dim)
        before = lax.ppermute(last, axis, up)
        after = lax.ppermute(first, axis, down)
        shard = jnp.concatenate([before, shard, after], axis=dim)
    return shard


def joined_along(tiles, dim):
    tiles = jnp.moveaxis(tiles, 0, dim)
    shape = tiles.shape
    return tiles.reshape(*shape[:dim], shape[dim] * shape[dim + 1], *shape[dim + 2 :])


def copy_for_each(shard, axis):
    copies = jnp.broadcast_to(shard, (lax.axis_size(axis), *shard.shape))
    return lax.all_to_all(copies, axis, split_axis=0, concat_axis=0, tiled=True)


def gather_directly(shard, axis, dim):
    return joined_along(copy_for_each(shard, axis), dim)


def over_copies(shard, axis):
    everything = copy_for_each(shard, axis)
    return jnp.sum(everything, axis=0)


def scale_rows(values, square_sum, width, gain):
    return values * lax.rsqrt(square_sum / width + norm_eps)[:, None] * gain


def band_attention(query_part, padded, sink_part, first_pos, seq_total):
    row_count = query_part.shape[0]
    blocks = row_count // WINDOW
    kv_heads = padded.shape[1] // (2 * HEAD_WIDTH)
    heads_per_group = query_part.shape[1] // (kv_heads * HEAD_WIDTH)
    query_tiles = query_part.reshape(blocks, WINDOW, kv_heads, heads_per_group, HEAD_WIDTH)
    kv_tiles = padded.reshape(blocks + 2, WINDOW, padded.shape[1])
    kv_band = jnp.concatenate([kv_tiles[:-2], kv_tiles[1:-1], kv_tiles[2:]], axis=1)
    key_band = kv_band[:, :, : kv_heads * HEAD_WIDTH].reshape(
        blocks, 3 * WINDOW, kv_heads, HEAD_WIDTH
    )
    value_band = kv_band[:, :, kv_heads * HEAD_WIDTH :].reshape(
        blocks, 3 * WINDOW, kv_heads, HEAD_WIDTH
    )
    scores = jnp.einsum(
        "nqhgd,nkhd->nhgqk", query_tiles, key_band, preferred_element_type=jnp.float32
    ) * HEAD_WIDTH ** (-0.5)
    block_start = first_pos + jnp.arange(blocks, dtype=jnp.int32)[:, None, None] * WINDOW
    query_pos = block_start + jnp.arange(WINDOW, dtype=jnp.int32)[None, :, None]
    key_pos = block_start - WINDOW + jnp.arange(3 * WINDOW, dtype=jnp.int32)[None, None, :]
    inside = (jnp.abs(query_pos - key_pos) <= WINDOW) & (key_pos >= 0) & (key_pos < seq_total)
    scores = jnp.where(inside[:, None, None], scores, -jnp.inf)
    sink_tiles = sink_part.reshape(kv_heads, heads_per_group)[None, :, :, None, None]
    row_max = jnp.maximum(jnp.max(scores, axis=-1, keepdims=True), sink_tiles)
    exp_scores = jnp.exp(scores - row_max)
    denominator = jnp.sum(exp_scores, axis=-1, keepdims=True) + jnp.exp(sink_tiles - row_max)
    weights = (exp_scores / denominator).astype(jnp.bfloat16)
    attn_out = jnp.einsum(
        "nhgqk,nkhd->nqhgd", weights, value_band, preferred_element_type=jnp.float32
    )
    return attn_out.reshape(row_count, query_part.shape[1]).astype(jnp.bfloat16)


def body(
    residual,
    rotated_query_rows,
    rotated_key_rows,
    value_matrix_rows,
    head_sink_logit,
    out_proj,
    gain_mix,
    gain_pre,
    gain_post,
    gate_proj,
    up_proj,
    down_proj,
):
    gate_all, up_all, down_all = rows_first((gate_proj, up_proj, down_proj), "sp", (0, 0, 1))
    row_count = rotated_query_rows.shape[0]
    first_pos = lax.axis_index("sp") * row_count
    seq_total = row_count * lax.axis_size("sp")
    col_count = residual.shape[1]
    col_start = lax.axis_index("tp") * col_count
    full_width = col_count * lax.axis_size("tp")
    kv_both = jnp.concatenate([rotated_key_rows, value_matrix_rows], axis=1)
    padded = with_halo(kv_both, (("sp", 0),), WINDOW)
    attended = band_attention(rotated_query_rows, padded, head_sink_logit, first_pos, seq_total)
    partial_value = jnp.dot(attended, out_proj, preferred_element_type=jnp.float32)
    own_gain_post = lax.dynamic_slice_in_dim(gain_post, col_start, col_count)
    mixed_share = lax.psum_scatter(
        partial_value.astype(jnp.bfloat16), "tp", scatter_dimension=1, tiled=True
    ).astype(jnp.float32)
    mixed_square = lax.psum(jnp.sum(mixed_share * mixed_share, axis=1), "tp")
    own_gain_mix = lax.dynamic_slice_in_dim(gain_mix, col_start, col_count)
    own_first = (
        residual.astype(jnp.float32)
        + scale_rows(mixed_share, mixed_square, full_width, own_gain_mix)
    ).astype(jnp.bfloat16)
    first_share = own_first.astype(jnp.float32)
    first_square = lax.psum(jnp.sum(first_share * first_share, axis=1), "tp")
    own_gain_pre = lax.dynamic_slice_in_dim(gain_pre, col_start, col_count)
    normed_share = scale_rows(first_share, first_square, full_width, own_gain_pre).astype(
        jnp.bfloat16
    )
    normed = gather_directly(normed_share, "tp", 1)
    gate_pre = jnp.dot(normed, gate_all, preferred_element_type=jnp.float32)
    up_pre = jnp.dot(normed, up_all, preferred_element_type=jnp.float32)
    hidden = (jax.nn.silu(gate_pre) * up_pre).astype(jnp.bfloat16)
    ffn_terms = jnp.dot(hidden, down_all, preferred_element_type=jnp.float32)
    ffn_share = lax.psum_scatter(
        ffn_terms.astype(jnp.bfloat16), "tp", scatter_dimension=1, tiled=True
    ).astype(jnp.float32)
    output_square = over_copies(jnp.sum(ffn_share * ffn_share, axis=1), "tp")
    return (
        own_first.astype(jnp.float32)
        + 0.5 * scale_rows(ffn_share, output_square, full_width, own_gain_post)
    ).astype(jnp.bfloat16)


def solution(mesh):
    placed = (
        P("sp", "tp"),
        P("sp", "tp"),
        P("sp", "tp"),
        P("sp", "tp"),
        P("tp"),
        P("tp", None),
        P(),
        P(),
        P(),
        P("sp", "tp"),
        P("sp", "tp"),
        P("tp", "sp"),
    )
    return jax.shard_map(body, mesh=mesh, in_specs=placed, out_specs=P("sp", "tp"), check_vma=False)
```

profile of v0, /device:TPU:0, one launch (start us, length us, event | category | flops | bytes accessed | tf_op | source)
XLA Modules:
  0.0 266.1 jit_solution(1520918387846533175)
XLA Ops:
  7.4 0.0 copy-start
  7.4 0.0 copy-start.6
  7.4 0.0 reduce-scatter.3.cloned.1.call-start
  7.4 1.1 constant_dynamic-update-slice_fusion.1
  8.5 1.0 constant_dynamic-update-slice_fusion
  9.5 1.3 collective-permute-start
  10.8 1.3 collective-permute-start.1
  12.2 0.1 fusion.37
  12.2 0.1 iota_add_fusion
  12.3 0.1 iota_add_fusion.1
  12.4 1.9 fusion.29
  14.2 1.0 copy.35
  15.2 2.3 copy.37
  17.5 1.3 copy.47
  18.8 0.0 copy-done.6
  18.8 0.1 max.18
  18.9 0.0 collective-permute-done
  18.9 0.0 collective-permute-done.1
  18.9 1.0 pad_maximum_fusion.3
  20.0 1.3 copy.34
  21.3 2.0 copy.36
  23.3 1.4 pad_maximum_fusion
  24.8 0.2 fusion.42
  24.9 1.7 fusion.1
  26.6 0.1 broadcast_maximum_fusion
  26.7 2.3 fusion
  29.0 0.1 exponential_add_fusion
  29.1 2.9 %fusion.31 = bf16[8,128,2,3,64]{1,4,3,2,0:T(8,128)(2,1)S(1)} fusion(bf16[8,384,2,64,1]{1,3,4,2,0:T(8,128)(2,1)S(1)} %bitcast.58, f32[8,2,384,128,3]{3,2,4,1,0:T(8,128)S(1)} %get-tuple-element.16, f32[8,2,3,128]{3,2,1,0:T(4,128)S(1)} %exponential_add_fusion, f32[8,2,3,128]{3,2,1,0:T(4,128)S(1)} %broadcast_maximum_fusion, pred[8,128,384]{1,2,0:T(8,128)(4,1)S(1)} %fusion.29), kind=kOutput, calls=%fused_computation.39 | convolution fusion | flops 314179584 | bytes 11452416 | tf_op jit(solution)/shard_map/nhgqk,nkhd->nqhgd/dot_general | solution.py:91
  32.0 0.5 copy.40
  32.6 0.0 copy-done
  32.6 4.4 %convolution_convert_fusion = bf16[1024,2048]{1,0:T(8,128)(2,1)} fusion(bf16[384,2048]{1,0:T(8,128)(2,1)S(1)} %copy-done, bf16[48,8,8,128]{3,2,1,0:T(8,128)(2,1)S(1)} %bitcast.57), kind=kOutput, calls=%fused_computation.13 | convolution fusion | flops 1612709888 | bytes 6553600 | tf_op jit(solution)/shard_map/dot_general | solution.py:121
  36.9 0.0 copy-start.3
  36.9 0.0 copy-start.4
  36.9 0.0 reduce-scatter.3.cloned.1.call-update
  37.0 0.0 all-gather.2.cloned.1.call-start
  37.0 0.8 copy-done.3
  37.8 0.1 copy-done.4
  37.9 0.1 copy-done.5
  38.0 0.9 pad_maximum_fusion.1
  38.9 0.0 all-gather.2.cloned.1.call-update
  38.9 0.0 reduce-scatter.5.cloned.1.call-start
  39.0 0.8 dynamic_slice.9
  39.7 0.8 dynamic_slice.10
  40.5 48.9 %reduce-scatter.3.cloned.1.call-done = bf16[1024,512]{1,0:T(8,128)(2,1)} async-done(((bf16[1024,2048]{1,0:T(8,128)(2,1)}), bf16[1024,512]{1,0:T(8,128)(2,1)}) %reduce-scatter.3.cloned.1.call-update) | async-done | bytes 1048592 | tf_op jit(solution)/shard_map/reduce_scatter | solution.py:123
  89.4 1.5 fusion.17
  90.9 8.6 %psum.14 = f32[1024]{0:T(1024)S(1)} all-reduce(f32[1024]{0:T(1024)S(1)} %fusion.17), channel_id=1, replica_groups=mesh['sp'=32,'tp'=4] {'tp'}, use_global_device_ids=true, to_apply=%region_4.5 | all-reduce | flops 1024 | bytes 8192 | tf_op jit(solution)/shard_map/psum | solution.py:126
  99.5 0.0 copy-done.2
  99.5 2.0 fusion.24
  101.5 9.0 %psum.15 = f32[1024]{0:T(1024)S(1)} all-reduce(f32[1024]{0:T(1024)S(1)} %get-tuple-element.5), channel_id=1, replica_groups=mesh['sp'=32,'tp'=4] {'tp'}, use_global_device_ids=true, to_apply=%region_6.7 | all-reduce | flops 1024 | bytes 8192 | tf_op jit(solution)/shard_map/psum | solution.py:133
  110.5 1.3 fusion.26
  111.8 1.6 copy.41
  113.4 0.5 broadcast_in_dim.18
  113.9 50.1 %all_to_all.11 = bf16[4,1024,512]{1,2,0:T(8,128)(2,1)} all-to-all(bf16[4,1024,512]{1,2,0:T(8,128)(2,1)S(1)} %broadcast_in_dim.18), channel_id=1, replica_groups=mesh['sp'=32,'tp'=4] {'tp'}, dimensions={0} | all-to-all | bytes 8388608 | tf_op jit(solution)/shard_map/all_to_all | solution.py:48
  164.0 11.8 %fusion.6 = f32[1024,1408]{1,0:T(8,128)} fusion(bf16[1024,2048]{0,1:T(8,128)(2,1)} %bitcast.49, bf16[2048,4224]{1,0:T(8,128)(2,1)} %all-gather.2.cloned.1.call-done), kind=kOutput, calls=%fused_computation.9 | convolution fusion | flops 5905580032 | bytes 15728640 | tf_op jit(solution)/shard_map/dot_general | solution.py:139
  175.8 23.1 %fusion.11 = bf16[1024,2048]{1,0:T(8,128)(2,1)} fusion(bf16[2048,4224]{1,0:T(8,128)(2,1)} %all-gather.2.cloned.1.call-done, f32[1024,1408]{1,0:T(8,128)} %fusion.6, bf16[1024,2048]{0,1:T(8,128)(2,1)} %bitcast.50), kind=kOutput, calls=%fused_computation.14 | convolution fusion | flops 11821907968 | bytes 25690112 | tf_op jit(solution)/shard_map/dot_general | solution.py:142
  198.9 0.0 reduce-scatter.5.cloned.1.call-update
  198.9 46.3 %reduce-scatter.5.cloned.1.call-done = bf16[1024,512]{1,0:T(8,128)(2,1)} async-done(((bf16[1024,2048]{1,0:T(8,128)(2,1)}), bf16[1024,512]{1,0:T(8,128)(2,1)}) %reduce-scatter.5.cloned.1.call-update) | async-done | bytes 1048592 | tf_op jit(solution)/shard_map/reduce_scatter | solution.py:143
  245.2 1.5 fusion.21
  246.7 0.6 broadcast_in_dim.19
  247.3 3.3 %all-to-all-start.1 = ((f32[4,1,1024]{2,1,0:T(1,128)}), f32[4,1,1024]{2,1,0:T(1,128)S(1)}, u32[]{:S(2)}, u32[]{:S(2)}) async-start(f32[4,1,1024]{2,1,0:T(1,128)} %broadcast_in_dim.19), calls=%async_computation.3 | async-start | bytes 32768 | tf_op jit(solution)/shard_map/all_to_all | solution.py:48
  250.6 0.8 dynamic_slice.11
  251.3 4.6 %all-to-all-done.1 = f32[4,1,1024]{2,1,0:T(1,128)S(1)} async-done(((f32[4,1,1024]{2,1,0:T(1,128)}), f32[4,1,1024]{2,1,0:T(1,128)S(1)}, u32[]{:S(2)}, u32[]{:S(2)}) %all-to-all-start.1) | async-done | bytes 16416 | tf_op jit(solution)/shard_map/all_to_all | solution.py:48
  255.9 2.7 %fusion.27 = bf16[1024,512]{1,0:T(8,128)(2,1)} fusion(bf16[1024,512]{1,0:T(8,128)(2,1)} %reduce-scatter.5.cloned.1.call-done, bf16[1024,512]{1,0:T(8,128)(2,1)S(1)} %get-tuple-element.6, f32[512]{0:T(512)S(1)} %dynamic_slice.11, f32[1024]{0:T(1024)S(1)} %add_rsqrt_fusion), kind=kLoop, calls=%fused_computation.33 | loop fusion | flops 3670016 | bytes 3151872 | tf_op jit(solution)/shard_map/convert_element_type | solution.py:150
  258.7 0.0 copy-done.1
  (10 shorter events, 0.1 us)
Async XLA Ops:
  7.4 25.2 %copy-start = (bf16[384,2048]{1,0:T(8,128)(2,1)S(1)}, bf16[384,2048]{1,0:T(8,128)(2,1)}, u32[]{:S(2)}) copy-start(bf16[384,2048]{1,0:T(8,128)(2,1)} %param.17) | copy-start | bytes 4718596
  7.4 11.5 %copy-start.6 = (f32[6]{0:T(128)S(1)}, f32[6]{0:T(128)}, u32[]{:S(2)}) copy-start(f32[6]{0:T(128)} %param.16) | copy-start | bytes 76
  7.4 82.0 %reduce-scatter.3.cloned.1.call-start = ((), (), s32[]{:S(2)}) async-start(), calls=%async_computation.4 | async-start | bytes 5242880 | tf_op jit(solution)/shard_map/reduce_scatter | solution.py:123
  9.5 9.4 %collective-permute-start = (bf16[128,256]{1,0:T(8,128)(2,1)S(1)}, bf16[128,256]{1,0:T(8,128)(2,1)S(1)}, u32[]{:S(2)}, u32[]{:S(2)}) collective-permute-start(bf16[128,256]{1,0:T(8,128)(2,1)S(1)} %get-tuple-element.11), channel_id=1, source_target_pairs={{0,4},{4,8},{8,12},{12,16},{16,20},{20,24},{24,28},{28,32},{32,36}... | collective-permute-start | bytes 196616 | tf_op jit(solution)/shard_map/ppermute | solution.py:34
  10.8 8.1 %collective-permute-start.1 = (bf16[128,256]{1,0:T(8,128)(2,1)S(1)}, bf16[128,256]{1,0:T(8,128)(2,1)S(1)}, u32[]{:S(2)}, u32[]{:S(2)}) collective-permute-start(bf16[128,256]{1,0:T(8,128)(2,1)S(1)} %get-tuple-element.12), channel_id=1, source_target_pairs={{4,0},{8,4},{12,8},{16,12},{20,16},{24,20},{28,24},{32,28},{36,32}... | collective-permute-start | bytes 196616 | tf_op jit(solution)/shard_map/ppermute | solution.py:35
  36.9 0.9 copy-start.3
  36.9 1.0 copy-start.4
  36.9 1.1 copy-start.5
  36.9 62.6 %copy-start.2 = (bf16[1024,512]{1,0:T(8,128)(2,1)S(1)}, bf16[1024,512]{1,0:T(8,128)(2,1)}, u32[]{:S(2)}) copy-start(bf16[1024,512]{1,0:T(8,128)(2,1)} %param.12) | copy-start | bytes 3145732
  37.0 127.0 %all-gather.2.cloned.1.call-start = ((), (), s32[]{:S(2)}) async-start(), calls=%async_computation.5 | async-start | bytes 17842176 | tf_op jit(solution)/shard_map/all_gather | solution.py:17
  38.9 206.3 %reduce-scatter.5.cloned.1.call-start = ((), (), s32[]{:S(2)}) async-start(), calls=%async_computation.6 | async-start | bytes 5242880 | tf_op jit(solution)/shard_map/reduce_scatter | solution.py:143
  198.9 59.7 %copy-start.1 = (bf16[384,2048]{1,0:T(8,128)(2,1)S(1)}, bf16[384,2048]{1,0:T(8,128)(2,1)}, u32[]{:S(2)}) copy-start(bf16[384,2048]{1,0:T(8,128)(2,1)} %param.17) | copy-start | bytes 4718596
  247.3 8.6 %all-to-all-start.1 = ((f32[4,1,1024]{2,1,0:T(1,128)}), f32[4,1,1024]{2,1,0:T(1,128)S(1)}, u32[]{:S(2)}, u32[]{:S(2)}) async-start(f32[4,1,1024]{2,1,0:T(1,128)} %broadcast_in_dim.19), calls=%async_computation.3 | async-start | bytes 32768 | tf_op jit(solution)/shard_map/all_to_all | solution.py:48
Sparse Core Ops, SparseCore 0:
  37.1 52.2 reduce-scatter.2
  199.1 46.0 reduce-scatter.4
Sparse Core Ops, SparseCore 1:
  39.7 79.3 all-gather.1
where the time goes:
time: 267 us; the launch traced here: 266 us
  waiting for transfers between devices  99.8 us (37%)
  blocking collectives  67.6 us (25%)
  matrix products  43.9 us (16%)
  local copies, waits for them, and re-layouts  16.9 us (6%)
  other arithmetic  16.9 us (6%)
  between operations  15 us (6%)
  starting transfers between devices  5.93 us (2%)
    all_to_all x1, blocking collectives, copy_for_each(): return lax.all_to_all(copies, axis, split_axis=0, concat_axis=0, tiled=True)  50.1 us
    reduce_scatter x1, waiting for transfers between devices, body(): lax.psum_scatter(partial_value.astype(jnp.bfloat16), 'tp', scatter_dimens...  48.9 us
    reduce_scatter x1, waiting for transfers between devices, body(): lax.psum_scatter(ffn_terms.astype(jnp.bfloat16), 'tp', scatter_dimension=...  46.3 us
    dot_general x1, matrix products, body(): ffn_terms = jnp.dot(hidden, down_all, preferred_element_type=jnp.float32)  23.1 us
    dot_general x1, matrix products, body(): gate_pre = jnp.dot(normed, gate_all, preferred_element_type=jnp.float32)  11.8 us
    psum x1, blocking collectives, body(): first_square = lax.psum(jnp.sum(first_share * first_share, axis=1), 'tp')  9 us
    psum x1, blocking collectives, body(): mixed_square = lax.psum(jnp.sum(mixed_share * mixed_share, axis=1), 'tp')  8.55 us
    unnamed x17, local copies, waits for them, and re-layouts  5.74 us
  transfers between devices with their start and end apart: 6, of which 3 were waited for; matrix products, arithmetic and copies ran while one was open for 6% of the time, Pallas kernels for 0%

commit v1 on v0

v1 whole, which is shorter than its diff:
```python
import functools

import jax
import jax.numpy as jnp
from jax import lax
from jax.experimental import pallas as pl
from jax.experimental.pallas import tpu as pltpu
from jax.sharding import PartitionSpec as P

WINDOW = 128
EPS = 1e-06
MESH = pl.DeviceIdType.MESH
F32 = jnp.float32
BF16 = jnp.bfloat16
NT = (((1,), (1,)), ((), ()))


def ring():
    me = lax.axis_index("tp")
    right, left, far = (lax.rem(me + k, 4) for k in (1, 3, 2))
    return me, right, left, far


def tp_copy(src, dst, send, recv, to):
    return pltpu.make_async_remote_copy(
        src_ref=src, dst_ref=dst, send_sem=send, recv_sem=recv,
        device_id={"tp": to}, device_id_type=MESH,
    )


def greet(barrier, others):
    for other in others:
        pl.semaphore_signal(barrier, inc=1, device_id=other, device_id_type=MESH)
    pl.semaphore_wait(barrier, len(others))


class Scatter:
    def __init__(self, sent, got, own, send, recv):
        self.sent, self.got, self.own, self.send, self.recv = sent, got, own, send, recv
        self.me, self.right, self.left, self.far = ring()

    def copy(self, slot, m):
        to = self.right if m % 2 == 0 else self.left
        return tp_copy(
            self.sent.at[slot, m], self.got.at[slot, m],
            self.send.at[slot, m], self.recv.at[slot, m], to,
        )

    def first(self, slot, part):
        self.sent[slot, 0] = part(self.far, 0)
        self.copy(slot, 0).start()
        self.sent[slot, 1] = part(self.far, 1)
        self.copy(slot, 1).start()
        self.sent[slot, 2] = part(self.right, 1)
        self.copy(slot, 2).start()
        self.sent[slot, 3] = part(self.left, 0)
        self.copy(slot, 3).start()
        self.sent[slot, 4] = part(self.right, 0)
        self.sent[slot, 5] = part(self.left, 1)
        self.own[slot, :, :256] = part(self.me, 0)
        self.own[slot, :, 256:] = part(self.me, 1)

    def second(self, slot):
        for k in (0, 1):
            self.copy(slot, k).wait_recv()
            total = self.sent[slot, 4 + k].astype(F32) + self.got[slot, k].astype(F32)
            self.sent[slot, 4 + k] = total.astype(BF16)
            self.copy(slot, 4 + k).start()

    def last(self, slot):
        for m in (2, 3, 4, 5):
            self.copy(slot, m).wait_recv()
        half0 = (
            self.own[slot, :, :256].astype(F32)
            + self.got[slot, 4].astype(F32)
            + self.got[slot, 3].astype(F32)
        )
        half1 = (
            self.own[slot, :, 256:].astype(F32)
            + self.got[slot, 2].astype(F32)
            + self.got[slot, 5].astype(F32)
        )
        return half0, half1

    def drain(self, slot):
        for m in range(6):
            self.copy(slot, m).wait_send()


class Squares:
    def __init__(self, mine, got, send, recv):
        self.mine, self.got, self.send, self.recv = mine, got, send, recv
        self.me, self.right, self.left, self.far = ring()

    def copies(self, slot):
        for m, to in enumerate((self.right, self.left, self.far)):
            yield tp_copy(
                self.mine.at[slot], self.got.at[slot, m],
                self.send.at[slot, m], self.recv.at[slot, m], to,
            )

    def give(self, slot, half0, half1):
        total = jnp.sum(half0 * half0, axis=1, keepdims=True) + jnp.sum(
            half1 * half1, axis=1, keepdims=True
        )
        for g in range(total.shape[0] // 128):
            wide = jnp.broadcast_to(total[128 * g : 128 * g + 128], (128, 128))
            self.mine[slot, 8 * g : 8 * g + 8] = wide.T[:8]
        for copy in self.copies(slot):
            copy.start()

    def take(self, slot):
        for copy in self.copies(slot):
            copy.wait_recv()
        total = self.mine[slot] + self.got[slot, 0] + self.got[slot, 1] + self.got[slot, 2]
        columns = [
            jnp.broadcast_to(total[8 * g : 8 * g + 1], (128, 128)).T[:, :1]
            for g in range(total.shape[0] // 8)
        ]
        return columns[0] if len(columns) == 1 else jnp.concatenate(columns, axis=0)

    def drain(self, slot):
        for copy in self.copies(slot):
            copy.wait_send()


def attend(row, first_key, q_ref, kv, sink_ref, lowest, highest):
    keys, keys_turned, values, values_turned = (
        a[pl.ds(first_key, 3 * WINDOW), :] for a in kv
    )
    lane = lax.broadcasted_iota(jnp.int32, (WINDOW, 128), 1)
    query = lax.broadcasted_iota(jnp.int32, (WINDOW, 3 * WINDOW), 0)
    key = lax.broadcasted_iota(jnp.int32, (WINDOW, 3 * WINDOW), 1)
    inside = (key >= query) & (key <= query + 2 * WINDOW) & (key >= lowest) & (key < highest)
    tiles = []
    for t in range(3):
        pair = q_ref[pl.ds(row, WINDOW), 128 * t : 128 * t + 128].astype(F32) * 0.125
        outs = []
        for half in range(2):
            h = 2 * t + half
            turned = (h // 3) != half
            q = jnp.where((lane >= 64) == (half == 1), pair, 0.0).astype(BF16)
            scores = lax.dot_general(
                q, keys_turned if turned else keys, NT, preferred_element_type=F32
            )
            scores = jnp.where(inside, scores, -1e30)
            sink = sink_ref[h]
            top = jnp.maximum(jnp.max(scores, axis=1, keepdims=True), sink)
            e = jnp.exp(scores - top)
            below = jnp.sum(e, axis=1, keepdims=True) + jnp.exp(sink - top)
            out = jnp.dot(
                e.astype(BF16), values_turned if turned else values,
                preferred_element_type=F32,
            )
            outs.append(out * (1.0 / below))
        tiles.append(jnp.where(lane < 64, outs[0], outs[1]).astype(BF16))
    return jnp.concatenate(tiles, axis=1)


def turn(x):
    return pltpu.roll(x.astype(F32), 64, 1).astype(BF16)


def mix_kernel(
    chunks, sp_count,
    res_ref, q_ref, k_ref, v_ref, sink_ref, proj_ref, gain_ref,
    out_ref,
    keys, keys_turned, values, values_turned, att,
    sent, got, own, mixed, mine, squares, rows,
    halo_send, halo_recv, rs_send, rs_recv, sq_send, sq_recv, ag_send, ag_recv,
):
    me, right, left, far = ring()
    sp = lax.axis_index("sp")
    after = lax.rem(sp + 1, sp_count)
    before = lax.rem(sp + sp_count - 1, sp_count)
    length = chunks * WINDOW
    greet(
        pltpu.get_barrier_semaphore(),
        [{"tp": right}, {"tp": left}, {"tp": far}, {"sp": after}, {"sp": before}],
    )

    def halo(n):
        mine_ref, whole = ((k_ref, keys), (v_ref, values))[n // 2]
        if n % 2 == 0:
            src, dst, to = mine_ref.at[pl.ds(length - WINDOW, WINDOW)], whole.at[pl.ds(0, WINDOW)], after
        else:
            src, dst, to = mine_ref.at[pl.ds(0, WINDOW)], whole.at[pl.ds(length + WINDOW, WINDOW)], before
        return pltpu.make_async_remote_copy(
            src_ref=src, dst_ref=dst, send_sem=halo_send.at[n], recv_sem=halo_recv.at[n],
            device_id={"sp": to}, device_id_type=MESH,
        )

    for n in range(4):
        halo(n).start()
    middle = pl.ds(WINDOW, length)
    keys[middle, :] = k_ref[...]
    values[middle, :] = v_ref[...]
    keys_turned[middle, :] = turn(k_ref[...])
    values_turned[middle, :] = turn(v_ref[...])

    scatter = Scatter(sent, got, own, rs_send, rs_recv)
    sums = Squares(mine, squares, sq_send, sq_recv)
    gain = gain_ref[:, pl.ds(pl.multiple_of(me * 512, 512), 512)]

    def place(slot):
        return lax.rem(slot + 1, chunks) * WINDOW

    def gather(slot, m):
        owner, to, part = (
            (me, right, pl.ds(0, 512)), (me, left, pl.ds(0, 512)),
            (left, right, pl.ds(0, 256)), (right, left, pl.ds(256, 256)),
        )[m]
        ref = rows.at[owner, slot, :, part]
        return tp_copy(ref, ref, ag_send.at[slot, m], ag_recv.at[slot, m], to)

    def arrived(slot, m):
        owner, part = (
            (left, pl.ds(0, 512)), (right, pl.ds(0, 512)),
            (far, pl.ds(0, 256)), (far, pl.ds(256, 256)),
        )[m]
        ref = rows.at[owner, slot, :, part]
        tp_copy(ref, ref, ag_send.at[slot, m], ag_recv.at[slot, m], right).wait_recv()

    def step(t, carry):
        @pl.when(t == chunks - 2)
        def _():
            for n in range(4):
                halo(n).wait_recv()
            for at in (0, length + WINDOW):
                keys_turned[pl.ds(at, WINDOW), :] = turn(keys[pl.ds(at, WINDOW), :])
                values_turned[pl.ds(at, WINDOW), :] = turn(values[pl.ds(at, WINDOW), :])

        @pl.when(t < chunks)
        def _():
            row = pl.multiple_of(place(t), WINDOW)
            lowest = jnp.where((sp == 0) & (t == chunks - 1), WINDOW, 0)
            highest = jnp.where((sp == sp_count - 1) & (t == chunks - 2), 2 * WINDOW, 3 * WINDOW)
            att[...] = attend(
                row, row, q_ref, (keys, keys_turned, values, values_turned),
                sink_ref, lowest, highest,
            )

            def part(block, half):
                columns = pl.ds(pl.multiple_of(block * 512 + 256 * half, 256), 256)
                return jnp.dot(
                    att[...], proj_ref[:, columns], preferred_element_type=F32
                ).astype(BF16)

            scatter.first(t, part)

        @pl.when((t >= 1) & (t < chunks + 1))
        def _():
            scatter.second(t - 1)

        @pl.when((t >= 2) & (t < chunks + 2))
        def _():
            half0, half1 = scatter.last(t - 2)
            mixed[t - 2, :, :256] = half0
            mixed[t - 2, :, 256:] = half1
            sums.give(t - 2, half0, half1)

        @pl.when((t >= 3) & (t < chunks + 3))
        def _():
            s = t - 3
            scale = lax.rsqrt(sums.take(s) / 2048.0 + EPS)
            res = res_ref[pl.ds(pl.multiple_of(place(s), WINDOW), WINDOW), :].astype(F32)
            rows[me, s] = (res + mixed[s] * scale * gain).astype(BF16)
            gather(s, 0).start()
            gather(s, 1).start()

        @pl.when((t >= 4) & (t < chunks + 4))
        def _():
            arrived(t - 4, 0)
            gather(t - 4, 2).start()
            arrived(t - 4, 1)
            gather(t - 4, 3).start()

        @pl.when(t >= 5)
        def _():
            arrived(t - 5, 2)
            arrived(t - 5, 3)

        return carry

    lax.fori_loop(0, chunks + 5, step, 0)

    for n in range(4):
        halo(n).wait_send()

    def drain(slot, carry):
        scatter.drain(slot)
        sums.drain(slot)
        for m in range(4):
            gather(slot, m).wait_send()
        return carry

    lax.fori_loop(0, chunks, drain, 0)
    out_ref[...] = rows[...]


def feed_kernel(
    chunks,
    rows_ref, gain_pre_ref, gain_post_ref, w_ref,
    out_ref,
    w_in, w_out, normed, hidden,
    sent, got, own, total, mine, squares,
    w_sem, rs_send, rs_recv, sq_send, sq_recv,
):
    me, right, left, far = ring()
    tiles = w_in.shape[1] // 256
    inner = w_in.shape[1]
    big = 2 * WINDOW

    def load(j):
        columns = pl.ds(pl.multiple_of(j * 256, 256), 256)
        return pltpu.make_async_copy(w_ref.at[:, columns], w_in.at[:, columns], w_sem.at[j])

    def load_out():
        return pltpu.make_async_copy(
            w_ref.at[:, pl.ds(inner, w_out.shape[1])], w_out, w_sem.at[tiles]
        )

    for j in range(tiles):
        load(j).start()
    load_out().start()
    greet(pltpu.get_barrier_semaphore(), [{"tp": right}, {"tp": left}, {"tp": far}])
    scatter = Scatter(sent, got, own, rs_send, rs_recv)
    sums = Squares(mine, squares, sq_send, sq_recv)
    gain = gain_post_ref[:, pl.ds(pl.multiple_of(me * 512, 512), 512)]

    def step(t, carry):
        @pl.when(t < chunks)
        def _():
            for k in range(2):
                squared = jnp.zeros((WINDOW, 1), F32)
                for b in range(4):
                    x = rows_ref[b, 2 * t + k].astype(F32)
                    squared += jnp.sum(x * x, axis=1, keepdims=True)
                scale = lax.rsqrt(squared / 2048.0 + EPS)
                for b in range(4):
                    x = rows_ref[b, 2 * t + k].astype(F32)
                    normed[WINDOW * k : WINDOW * k + WINDOW, 512 * b : 512 * b + 512] = (
                        x * scale * gain_pre_ref[:, 512 * b : 512 * b + 512]
                    ).astype(BF16)

            def tile(j, carry):
                @pl.when(t == 0)
                def _():
                    load(j).wait()

                both = jnp.dot(
                    normed[...], w_in[:, pl.ds(pl.multiple_of(j * 256, 256), 256)],
                    preferred_element_type=F32,
                )
                gate, up = both[:, :128], both[:, 128:]
                hidden[:, pl.ds(pl.multiple_of(j * 128, 128), 128)] = (
                    gate / (1.0 + jnp.exp(-gate)) * up
                ).astype(BF16)
                return carry

            lax.fori_loop(0, tiles, tile, 0)

            @pl.when(t == 0)
            def _():
                load_out().wait()

            def part(block, half):
                at = pl.ds(pl.multiple_of(block * 512 + 256 * half, 256), 256)
                return lax.dot_general(
                    hidden[...], w_out[at, :], NT, preferred_element_type=F32
                ).astype(BF16)

            scatter.first(t, part)

        @pl.when((t >= 1) & (t < chunks + 1))
        def _():
            scatter.second(t - 1)

        @pl.when((t >= 2) & (t < chunks + 2))
        def _():
            half0, half1 = scatter.last(t - 2)
            total[t - 2, :, :256] = half0
            total[t - 2, :, 256:] = half1
            sums.give(t - 2, half0, half1)

        @pl.when(t >= 3)
        def _():
            s = t - 3
            scale = lax.rsqrt(sums.take(s) / 2048.0 + EPS)
            for k in range(2):
                part = pl.ds(WINDOW * k, WINDOW)
                row = pl.multiple_of(lax.rem(2 * s + k + 1, 2 * chunks) * WINDOW, WINDOW)
                out_ref[pl.ds(row, WINDOW), :] = (
                    rows_ref[me, 2 * s + k].astype(F32)
                    + 0.5 * (total[s, part, :] * scale[WINDOW * k : WINDOW * k + WINDOW] * gain)
                ).astype(BF16)

        return carry

    lax.fori_loop(0, chunks + 3, step, 0)

    def drain(slot, carry):
        scatter.drain(slot)
        sums.drain(slot)
        return carry

    lax.fori_loop(0, chunks, drain, 0)


def sems(*shapes):
    return [pltpu.SemaphoreType.DMA(s) for s in shapes]


def body(
    residual, rotated_query_rows, rotated_key_rows, value_matrix_rows, head_sink_logit,
    out_proj, gain_mix, gain_pre, gain_post, gate_proj, up_proj, down_proj,
):
    length = residual.shape[0]
    chunks = length // WINDOW
    depth, units = gate_proj.shape
    both = jnp.stack(
        [gate_proj.reshape(depth, units // 128, 128), up_proj.reshape(depth, units // 128, 128)],
        axis=2,
    ).reshape(depth, 2 * units)
    weights = lax.all_gather(
        jnp.concatenate([both, down_proj.T], axis=1), "sp", axis=0, tiled=True
    )
    vmem = pl.BlockSpec(memory_space=pltpu.VMEM)
    rows = pl.pallas_call(
        functools.partial(mix_kernel, chunks, lax.axis_size("sp")),
        out_shape=jax.ShapeDtypeStruct((4, chunks, WINDOW, 512), BF16),
        in_specs=[vmem] * 4 + [pl.BlockSpec(memory_space=pltpu.SMEM)] + [vmem] * 2,
        out_specs=vmem,
        scratch_shapes=[pltpu.VMEM((length + 2 * WINDOW, 128), BF16)] * 4
        + [
            pltpu.VMEM((WINDOW, 384), BF16),
            pltpu.VMEM((chunks, 6, WINDOW, 256), BF16),
            pltpu.VMEM((chunks, 6, WINDOW, 256), BF16),
            pltpu.VMEM((chunks, WINDOW, 512), BF16),
            pltpu.VMEM((chunks, WINDOW, 512), F32),
            pltpu.VMEM((chunks, 8, 128), F32),
            pltpu.VMEM((chunks, 3, 8, 128), F32),
            pltpu.VMEM((4, chunks, WINDOW, 512), BF16),
        ]
        + sems((4,), (4,), (chunks, 6), (chunks, 6), (chunks, 3), (chunks, 3), (chunks, 4), (chunks, 4)),
        compiler_params=pltpu.CompilerParams(
            collective_id=0, has_side_effects=True, vmem_limit_bytes=40 * 2**20
        ),
        cost_estimate=pl.CostEstimate(
            flops=50 * 10**9, bytes_accessed=8 * 2**20, transcendentals=0
        ),
    )(
        residual, rotated_query_rows, rotated_key_rows, value_matrix_rows, head_sink_logit,
        out_proj, gain_mix[None],
    )
    half = chunks // 2
    big = 2 * WINDOW
    full = weights.shape[0]
    return pl.pallas_call(
        functools.partial(feed_kernel, half),
        out_shape=jax.ShapeDtypeStruct(residual.shape, BF16),
        in_specs=[vmem] * 3 + [pl.BlockSpec(memory_space=pl.ANY)],
        out_specs=vmem,
        scratch_shapes=[
            pltpu.VMEM((full, 2 * units), BF16),
            pltpu.VMEM((full, units), BF16),
            pltpu.VMEM((big, full), BF16),
            pltpu.VMEM((big, units), BF16),
            pltpu.VMEM((half, 6, big, 256), BF16),
            pltpu.VMEM((half, 6, big, 256), BF16),
            pltpu.VMEM((half, big, 512), BF16),
            pltpu.VMEM((half, big, 512), F32),
            pltpu.VMEM((half, 16, 128), F32),
            pltpu.VMEM((half, 3, 16, 128), F32),
        ]
        + sems((2 * units // 256 + 1,), (half, 6), (half, 6), (half, 3), (half, 3)),
        compiler_params=pltpu.CompilerParams(
            collective_id=1, has_side_effects=True, vmem_limit_bytes=60 * 2**20
        ),
    )(rows, gain_pre[None], gain_post[None], weights)


def solution(mesh):
    placed = (
        P("sp", "tp"), P("sp", "tp"), P("sp", "tp"), P("sp", "tp"), P("tp"), P("tp", None),
        P(), P(), P(), P("sp", "tp"), P("sp", "tp"), P("tp", "sp"),
    )
    return jax.shard_map(body, mesh=mesh, in_specs=placed, out_specs=P("sp", "tp"), check_vma=False)
```

time: 267 us -> 165 us (0.62)
  Pallas kernels: 0 us -> 138 us
  waiting for transfers between devices: 99.8 us -> 0.02 us
  blocking collectives: 67.6 us -> 0 us
  matrix products: 43.9 us -> 0 us
  other arithmetic: 16.9 us -> 2.02 us
  starting transfers between devices: 5.93 us -> 0.01 us
  local copies, waits for them, and re-layouts: 16.9 us -> 11.2 us
    pallas_call x0 -> x2, Pallas kernels: none -> 138 us  [the longest x1 82.4 us: body(): pl.pallas_call(functools.partial(mix_kernel, chunks, lax.axis_size('sp'))...]
    reduce_scatter x2 -> x0, waiting for transfers between devices: 95.2 us -> none  [the longest x1 48.9 us: body(): lax.psum_scatter(partial_value.astype(jnp.bfloat16), 'tp', scatter_dimens...]
    all_to_all x1 -> x0, blocking collectives: 50.1 us -> none  [copy_for_each(): return lax.all_to_all(copies, axis, split_axis=0, concat_axis=0, tiled=True)]
    dot_general x5 -> x0, matrix products: 43.9 us -> none  [the longest x1 23.1 us: body(): ffn_terms = jnp.dot(hidden, down_all, preferred_element_type=jnp.float32)]
    psum x2 -> x0, blocking collectives: 17.5 us -> none  [the longest x1 9 us: body(): first_square = lax.psum(jnp.sum(first_share * first_share, axis=1), 'tp')]
    reduce_sum x5 -> x0, other arithmetic: 7.35 us -> none  [the longest x1 2.32 us: band_attention(): jnp.sum(exp_scores, axis=-1, keepdims=True) + jnp.exp(sink_tiles - row_max)]
    all_to_all x1 -> x0, waiting for transfers between devices: 4.56 us -> none  [copy_for_each(): return lax.all_to_all(copies, axis, split_axis=0, concat_axis=0, tiled=True)]
    slice x5 -> x0, local copies, waits for them, and re-layouts: 4.54 us -> none  [the longest x1 2.04 us: band_attention(): kv_tiles[2:]]
  transfers between devices with their start and end apart: 6 -> 1, of which waited for: 3 -> 0; matrix products, arithmetic and copies ran while one was open for 6% -> 0% of each run, Pallas kernels for 0% -> 50%
where the time goes in v1:
time: 165 us; the launch traced here: 164 us
  Pallas kernels  138 us (84%)
  between operations  13.5 us (8%)
  local copies, waits for them, and re-layouts  11.2 us (7%)
  other arithmetic  2.02 us (1%)
    pallas_call x1, Pallas kernels, body(): pl.pallas_call(functools.partial(mix_kernel, chunks, lax.axis_size('sp'))...  82.4 us
    pallas_call x1, Pallas kernels, body(): pl.pallas_call(functools.partial(feed_kernel, half), out_shape=jax.ShapeD...  55.3 us
    unnamed x17, local copies, waits for them, and re-layouts  6.17 us
  transfers between devices with their start and end apart: 1, of which 0 were waited for; matrix products, arithmetic and copies ran while one was open for 0% of the time, Pallas kernels for 50%

profile of v1, /device:TPU:0, one launch (start us, length us, event | category | flops | bytes accessed | tf_op | source)
XLA Modules:
  0.0 164.5 jit_solution(7922442257441266525)
XLA Ops:
  6.5 0.0 all-gather.2.cloned.1.call-start
  6.5 1.0 stack_reshape.6
  7.6 1.1 stack_reshape.7
  8.6 0.0 copy-start.3
  8.7 0.1 pad_maximum_fusion.1
  8.8 0.0 copy-start.1
  8.8 0.0 copy-start.2
  8.8 0.0 copy-start.6
  8.8 0.0 copy-start.7
  8.8 1.1 copy.15
  9.9 1.9 %reshape.3 = bf16[64,2816]{1,0:T(8,128)(2,1)} reshape(bf16[64,11,2,128]{3,2,1,0:T(2,128)(2,1)} %copy.15) | data formatting | bytes 720896 | tf_op jit(solution)/shard_map/reshape | solution.py:424
  11.8 1.9 %pad_maximum_fusion = bf16[64,4224]{1,0:T(8,128)(2,1)} fusion(bf16[64,1408]{1,0:T(8,128)(2,1)} %bitcast.5, bf16[64,2816]{1,0:T(8,128)(2,1)} %reshape.3), kind=kLoop, calls=%fused_computation | loop fusion | flops 1081344 | bytes 1081344 | tf_op jit(solution)/shard_map/concatenate | solution.py:426
  13.7 0.0 all-gather.2.cloned.1.call-update
  13.7 0.0 copy-done.3
  13.7 0.0 copy-done.1
  13.8 0.0 copy-done.2
  13.8 0.0 copy-done.6
  13.8 0.0 copy-done.7
  13.8 0.0 copy-start.4
  13.8 0.9 copy-done.4
  14.7 0.0 copy-start.5
  14.7 0.9 copy-done.5
  15.7 82.4 %shard_map.118.rows_ref = bf16[4,8,128,512]{3,2,1,0:T(8,128)(2,1)S(1)} custom-call(bf16[1024,512]{1,0:T(8,128)(2,1)S(1)} %copy-done.2, bf16[1024,384]{1,0:T(8,128)(2,1)S(1)} %copy-done.3, bf16[1024,128]{1,0:T(8,128)(2,1)S(1)} %copy-done.4, bf16[1024,128]{1,0:T(8,128)(2,1)S(1)} %copy-done.5, f32[6]{0:T(128)S(1)} %copy-done.7, ...), custom_call_target="tpu_custom_call" | custom-call | flops 49999998976 | bytes 8388608 | tf_op jit(solution)/shard_map/pallas_call | solution.py:429
  98.1 0.0 copy-start
  98.1 2.0 %copy-done = bf16[4,8,128,512]{3,2,1,0:T(8,128)(2,1)} copy-done((bf16[4,8,128,512]{3,2,1,0:T(8,128)(2,1)}, bf16[4,8,128,512]{3,2,1,0:T(8,128)(2,1)S(1)}, u32[]{:S(2)}) %copy-start) | copy-done | bytes 4194328
  100.1 0.0 all-gather.2.cloned.1.call-done.w_ref
  100.1 55.3 %shard_map.119 = bf16[1024,512]{1,0:T(8,128)(2,1)} custom-call(bf16[4,8,128,512]{3,2,1,0:T(8,128)(2,1)} %copy-done, f32[1,2048]{1,0:T(1,128)} %bitcast.6, f32[1,2048]{1,0:T(1,128)} %bitcast.7, bf16[2048,4224]{1,0:T(8,128)(2,1)} %all-gather.2.cloned.1.call-done.w_ref), custom_call_target="tpu_custom_call" | custom-call | tf_op jit(solution)/shard_map/pallas_call | solution.py:459
  155.4 2.3 %copy.17 = bf16[1024,512]{1,0:T(8,128)(2,1)} copy(bf16[1024,512]{1,0:T(8,128)(2,1)} %shard_map.119) | data formatting | bytes 2097152
Async XLA Ops:
  6.5 93.6 %all-gather.2.cloned.1.call-start = ((), (), s32[]{:S(2)}) async-start(), calls=%async_computation | async-start | bytes 17842176 | tf_op jit(solution)/shard_map/all_gather | solution.py:425
  8.6 5.1 %copy-start.3 = (bf16[1024,384]{1,0:T(8,128)(2,1)S(1)}, bf16[1024,384]{1,0:T(8,128)(2,1)}, u32[]{:S(2)}) copy-start(bf16[1024,384]{1,0:T(8,128)(2,1)} %q_ref.1) | copy-start | bytes 2359300
  8.8 5.0 %copy-start.1 = (bf16[384,2048]{1,0:T(8,128)(2,1)S(1)}, bf16[384,2048]{1,0:T(8,128)(2,1)}, u32[]{:S(2)}) copy-start(bf16[384,2048]{1,0:T(8,128)(2,1)} %proj_ref.1) | copy-start | bytes 4718596
  8.8 5.0 %copy-start.2 = (bf16[1024,512]{1,0:T(8,128)(2,1)S(1)}, bf16[1024,512]{1,0:T(8,128)(2,1)}, u32[]{:S(2)}) copy-start(bf16[1024,512]{1,0:T(8,128)(2,1)} %res_ref.1) | copy-start | bytes 3145732
  8.8 5.0 %copy-start.6 = (f32[2048]{0:T(1024)S(1)}, f32[2048]{0:T(1024)}, u32[]{:S(2)}) copy-start(f32[2048]{0:T(1024)} %param.18) | copy-start | bytes 24580
  8.8 5.0 %copy-start.7 = (f32[6]{0:T(128)S(1)}, f32[6]{0:T(128)}, u32[]{:S(2)}) copy-start(f32[6]{0:T(128)} %sink_ref.1) | copy-start | bytes 76
  13.8 1.0 copy-start.4
  14.7 0.9 copy-start.5
  98.1 2.0 %copy-start = (bf16[4,8,128,512]{3,2,1,0:T(8,128)(2,1)}, bf16[4,8,128,512]{3,2,1,0:T(8,128)(2,1)S(1)}, u32[]{:S(2)}) copy-start(bf16[4,8,128,512]{3,2,1,0:T(8,128)(2,1)S(1)} %shard_map.118.rows_ref) | copy-start | bytes 12582916
Sparse Core Ops, SparseCore 0:
  13.9 76.2 all-gather.1

commit v2 on v1

v2 whole, which is shorter than its diff:
```python
import functools

import jax
import jax.numpy as jnp
from jax import lax
from jax.experimental import pallas as pl
from jax.experimental.pallas import tpu as pltpu
from jax.sharding import PartitionSpec as P

WINDOW = 128
EPS = 1e-06
FEED_AT = 8
MESH = pl.DeviceIdType.MESH
F32 = jnp.float32
BF16 = jnp.bfloat16
NT = (((1,), (1,)), ((), ()))


def ring():
    me = lax.axis_index("tp")
    right, left, far = (lax.rem(me + k, 4) for k in (1, 3, 2))
    return me, right, left, far


def tp_copy(src, dst, send, recv, to):
    return pltpu.make_async_remote_copy(
        src_ref=src, dst_ref=dst, send_sem=send, recv_sem=recv,
        device_id={"tp": to}, device_id_type=MESH,
    )


class Scatter:
    def __init__(self, sent, got, own, send, recv):
        self.sent, self.got, self.own, self.send, self.recv = sent, got, own, send, recv
        self.me, self.right, self.left, self.far = ring()

    def copy(self, slot, m):
        to = self.right if m % 2 == 0 else self.left
        return tp_copy(
            self.sent.at[slot, m], self.got.at[slot, m],
            self.send.at[slot, m], self.recv.at[slot, m], to,
        )

    def first(self, slot, part):
        self.sent[slot, 0] = part(self.far, 0)
        self.copy(slot, 0).start()
        self.sent[slot, 1] = part(self.far, 1)
        self.copy(slot, 1).start()
        self.sent[slot, 2] = part(self.right, 1)
        self.copy(slot, 2).start()
        self.sent[slot, 3] = part(self.left, 0)
        self.copy(slot, 3).start()
        self.sent[slot, 4] = part(self.right, 0)
        self.sent[slot, 5] = part(self.left, 1)
        self.own[slot, :, :256] = part(self.me, 0)
        self.own[slot, :, 256:] = part(self.me, 1)

    def second(self, slot):
        for k in (0, 1):
            self.copy(slot, k).wait_recv()
            total = self.sent[slot, 4 + k].astype(F32) + self.got[slot, k].astype(F32)
            self.sent[slot, 4 + k] = total.astype(BF16)
            self.copy(slot, 4 + k).start()

    def last(self, slot):
        for m in (2, 3, 4, 5):
            self.copy(slot, m).wait_recv()
        half0 = (
            self.own[slot, :, :256].astype(F32)
            + self.got[slot, 4].astype(F32)
            + self.got[slot, 3].astype(F32)
        )
        half1 = (
            self.own[slot, :, 256:].astype(F32)
            + self.got[slot, 2].astype(F32)
            + self.got[slot, 5].astype(F32)
        )
        return half0, half1

    def drain(self, slot):
        for m in range(6):
            self.copy(slot, m).wait_send()


class Squares:
    def __init__(self, mine, got, send, recv):
        self.mine, self.got, self.send, self.recv = mine, got, send, recv
        self.me, self.right, self.left, self.far = ring()

    def copies(self, slot):
        for m, to in enumerate((self.right, self.left, self.far)):
            yield tp_copy(
                self.mine.at[slot], self.got.at[slot, m],
                self.send.at[slot, m], self.recv.at[slot, m], to,
            )

    def give(self, slot, half0, half1):
        total = jnp.sum(half0 * half0, axis=1, keepdims=True) + jnp.sum(
            half1 * half1, axis=1, keepdims=True
        )
        for g in range(total.shape[0] // 128):
            wide = jnp.broadcast_to(total[128 * g : 128 * g + 128], (128, 128))
            self.mine[slot, 8 * g : 8 * g + 8] = wide.T[:8]
        for copy in self.copies(slot):
            copy.start()

    def take(self, slot):
        for copy in self.copies(slot):
            copy.wait_recv()
        total = self.mine[slot] + self.got[slot, 0] + self.got[slot, 1] + self.got[slot, 2]
        columns = [
            jnp.broadcast_to(total[8 * g : 8 * g + 1], (128, 128)).T[:, :1]
            for g in range(total.shape[0] // 8)
        ]
        return columns[0] if len(columns) == 1 else jnp.concatenate(columns, axis=0)

    def drain(self, slot):
        for copy in self.copies(slot):
            copy.wait_send()


def attend(row, first_key, q_ref, kv, sink_ref, lowest, highest):
    keys, keys_turned, values, values_turned = (
        a[pl.ds(first_key, 3 * WINDOW), :] for a in kv
    )
    lane = lax.broadcasted_iota(jnp.int32, (WINDOW, 128), 1)
    query = lax.broadcasted_iota(jnp.int32, (WINDOW, 3 * WINDOW), 0)
    key = lax.broadcasted_iota(jnp.int32, (WINDOW, 3 * WINDOW), 1)
    inside = (key >= query) & (key <= query + 2 * WINDOW) & (key >= lowest) & (key < highest)
    tiles = []
    for t in range(3):
        pair = q_ref[pl.ds(row, WINDOW), 128 * t : 128 * t + 128].astype(F32) * 0.125
        outs = []
        for half in range(2):
            h = 2 * t + half
            turned = (h // 3) != half
            q = jnp.where((lane >= 64) == (half == 1), pair, 0.0).astype(BF16)
            scores = lax.dot_general(
                q, keys_turned if turned else keys, NT, preferred_element_type=F32
            )
            scores = jnp.where(inside, scores, -1e30)
            sink = sink_ref[h]
            top = jnp.maximum(jnp.max(scores, axis=1, keepdims=True), sink)
            e = jnp.exp(scores - top)
            below = jnp.sum(e, axis=1, keepdims=True) + jnp.exp(sink - top)
            out = jnp.dot(
                e.astype(BF16), values_turned if turned else values,
                preferred_element_type=F32,
            )
            outs.append(out * (1.0 / below))
        tiles.append(jnp.where(lane < 64, outs[0], outs[1]).astype(BF16))
    return jnp.concatenate(tiles, axis=1)


def turn(x):
    return pltpu.roll(x.astype(F32), 64, 1).astype(BF16)


class Weights:
    across = (0, 1, 3, 2)

    def __init__(self, whole, send, recv, core_send, core_recv):
        self.whole, self.send, self.recv = whole, send, recv
        self.core_send, self.core_recv = core_send, core_recv
        sp = lax.axis_index("sp")
        self.core, self.y, self.z = lax.rem(sp, 2), lax.rem(lax.div(sp, 2), 4), lax.div(sp, 8)

    def device(self, way, a, b, core):
        dy, dz = (a, b) if way == 0 else (b, a)
        return (lax.rem(self.z + dz, 4) * 4 + lax.rem(self.y + dy, 4)) * 2 + core

    def neighbours(self):
        ring = [self.device(0, a, b, self.core) for a, b in ((1, 0), (3, 0), (0, 1), (0, 3))]
        return ring + [self.device(0, 0, 0, 1 - self.core)]

    def rows(self, way, a, b, core, part=None):
        start = self.device(way, a, b, core) * 64 + 32 * way
        if part is None:
            return self.whole.at[pl.ds(pl.multiple_of(start, 32), 32), :]
        return self.whole.at[pl.ds(pl.multiple_of(start + 16 * part, 16), 16), :]

    def at(self, stage, k):
        return (k, 0) if stage == 0 else (self.across[stage - 1], k)

    def copy(self, way, stage, m, incoming=False):
        offset = ((3, 1, 2, 2) if incoming else (0, 0, 3, 1))[m]
        ref = self.rows(way, *self.at(stage, offset), self.core, None if m < 2 else m - 2)
        to = self.device(way, *((1 if m % 2 == 0 else 3, 0) if stage == 0 else (0, 1 if m % 2 == 0 else 3)), self.core)
        return pltpu.make_async_remote_copy(
            src_ref=ref, dst_ref=ref,
            send_sem=self.send.at[way, stage, m], recv_sem=self.recv.at[way, stage, m],
            device_id={"sp": to}, device_id_type=MESH,
        )

    def over(self, way, a, b, incoming=False):
        ref = self.rows(way, a, b, 1 - self.core if incoming else self.core)
        return pltpu.make_async_remote_copy(
            src_ref=ref, dst_ref=ref,
            send_sem=self.core_send.at[way, 4 * a + b], recv_sem=self.core_recv.at[way, 4 * a + b],
            device_id={"sp": self.device(way, 0, 0, 1 - self.core)}, device_id_type=MESH,
        )

    def open(self, way, stage):
        self.copy(way, stage, 0).start()
        self.copy(way, stage, 1).start()

    def relay(self, way, stage):
        for m in (0, 1):
            self.copy(way, stage, m, True).wait_recv()
            self.copy(way, stage, m + 2).start()

    def share(self, way, stage, ks):
        for k in ks:
            self.over(way, *self.at(stage, k)).start()

    def close(self, way, stage):
        for m in (2, 3):
            self.copy(way, stage, m, True).wait_recv()
        self.share(way, stage, (2,))

    def step(self, n):
        for way in (0, 1):
            if n == 0:
                self.open(way, 0)
            elif n == 1:
                self.relay(way, 0)
        for way in (0, 1):
            if n == 0:
                self.open(way, 1)
                self.over(way, 0, 0).start()
            elif n == 1:
                self.open(way, 2)
                self.open(way, 3)
                self.share(way, 0, (1, 3))
            elif n == 2:
                self.relay(way, 1)
                self.share(way, 1, (1, 3))
            elif n == 3:
                self.close(way, 0)
                self.open(way, 4)
            elif n == 4:
                for stage in (2, 3):
                    self.relay(way, stage)
                    self.share(way, stage, (1, 3))
            elif n == 5:
                self.close(way, 1)
                self.relay(way, 4)
                self.share(way, 4, (1, 3))
            elif n == 6:
                for stage in (2, 3, 4):
                    self.close(way, stage)
            elif n == 7:
                for a in range(4):
                    for b in range(4):
                        self.over(way, a, b, True).wait_recv()

    def drain(self):
        for way in (0, 1):
            for stage in range(5):
                for m in range(4):
                    self.copy(way, stage, m).wait_send()
            for a in range(4):
                for b in range(4):
                    self.over(way, a, b).wait_send()


def layer_kernel(
    chunks, sp_count,
    res_hbm, q_hbm, k_hbm, v_hbm, sink_ref, proj_hbm, gain_mix_ref, gain_pre_ref, gain_post_ref,
    gate_hbm, up_hbm, down_hbm,
    out_ref,
    res_ref, q_ref, k_ref, v_ref, proj_ref, gate_ref, up_ref, down_ref,
    whole, keys, keys_turned, values, values_turned, att,
    sent, got, own, mixed, mine, squares, rows,
    normed, hidden, f_sent, f_got, f_own, f_total, f_mine, f_squares,
    load_sem, w_send, w_recv, core_send, core_recv,
    halo_send, halo_recv, rs_send, rs_recv, sq_send, sq_recv, ag_send, ag_recv,
    f_rs_send, f_rs_recv, f_sq_send, f_sq_recv,
):
    me, right, left, far = ring()
    sp = lax.axis_index("sp")
    after = lax.rem(sp + 1, sp_count)
    before = lax.rem(sp + sp_count - 1, sp_count)
    length = chunks * WINDOW
    half_chunks = chunks // 2
    units = gate_ref.shape[1]
    tiles = units // 128
    inner = 2 * units
    loads = [
        pltpu.make_async_copy(a, b, load_sem.at[n])
        for n, (a, b) in enumerate((
            (gate_hbm, gate_ref), (up_hbm, up_ref), (down_hbm, down_ref), (k_hbm, k_ref),
            (v_hbm, v_ref), (q_hbm, q_ref), (proj_hbm, proj_ref), (res_hbm, res_ref),
        ))
    ]
    for load in loads:
        load.start()
    weights = Weights(whole, w_send, w_recv, core_send, core_recv)
    barrier = pltpu.get_barrier_semaphore()
    others = [{"tp": right}, {"tp": left}, {"tp": far}, {"sp": after}, {"sp": before}]
    others += [{"sp": n} for n in weights.neighbours()]
    for other in others:
        pl.semaphore_signal(barrier, inc=1, device_id=other, device_id_type=MESH)
    for load in loads[:3]:
        load.wait()
    shard = pl.ds(pl.multiple_of(sp * 64, 64), 64)
    for j in range(tiles):
        whole[shard, 256 * j : 256 * j + 128] = gate_ref[:, 128 * j : 128 * j + 128]
        whole[shard, 256 * j + 128 : 256 * j + 256] = up_ref[:, 128 * j : 128 * j + 128]
        whole[shard, inner + 128 * j : inner + 128 * j + 128] = (
            down_ref[128 * j : 128 * j + 128, :].astype(F32).T.astype(BF16)
        )
    for load in loads[3:5]:
        load.wait()
    pl.semaphore_wait(barrier, len(others))

    def halo(n):
        mine_ref, both = ((k_ref, keys), (v_ref, values))[n // 2]
        if n % 2 == 0:
            src, dst, to = mine_ref.at[pl.ds(length - WINDOW, WINDOW)], both.at[pl.ds(0, WINDOW)], after
        else:
            src, dst, to = mine_ref.at[pl.ds(0, WINDOW)], both.at[pl.ds(length + WINDOW, WINDOW)], before
        return pltpu.make_async_remote_copy(
            src_ref=src, dst_ref=dst, send_sem=halo_send.at[n], recv_sem=halo_recv.at[n],
            device_id={"sp": to}, device_id_type=MESH,
        )

    for n in range(4):
        halo(n).start()
    weights.step(0)
    middle = pl.ds(WINDOW, length)
    keys[middle, :] = k_ref[...]
    values[middle, :] = v_ref[...]
    keys_turned[middle, :] = turn(k_ref[...])
    values_turned[middle, :] = turn(v_ref[...])
    for load in loads[5:]:
        load.wait()

    scatter = Scatter(sent, got, own, rs_send, rs_recv)
    sums = Squares(mine, squares, sq_send, sq_recv)
    f_scatter = Scatter(f_sent, f_got, f_own, f_rs_send, f_rs_recv)
    f_sums = Squares(f_mine, f_squares, f_sq_send, f_sq_recv)
    columns = pl.ds(pl.multiple_of(me * 512, 512), 512)
    gain_mix = gain_mix_ref[:, columns]
    gain_post = gain_post_ref[:, columns]

    def place(slot):
        return pl.multiple_of(lax.rem(slot + 1, chunks) * WINDOW, WINDOW)

    def gather(slot, m):
        owner, to, part = (
            (me, right, pl.ds(0, 512)), (me, left, pl.ds(0, 512)),
            (left, right, pl.ds(0, 256)), (right, left, pl.ds(256, 256)),
        )[m]
        ref = rows.at[owner, slot, :, part]
        return tp_copy(ref, ref, ag_send.at[slot, m], ag_recv.at[slot, m], to)

    def arrived(slot, m):
        owner, part = (
            (left, pl.ds(0, 512)), (right, pl.ds(0, 512)),
            (far, pl.ds(0, 256)), (far, pl.ds(256, 256)),
        )[m]
        ref = rows.at[owner, slot, :, part]
        tp_copy(ref, ref, ag_send.at[slot, m], ag_recv.at[slot, m], right).wait_recv()

    def attention(t):
        @pl.when(t == chunks - 2)
        def _():
            for n in range(4):
                halo(n).wait_recv()
            for at in (0, length + WINDOW):
                keys_turned[pl.ds(at, WINDOW), :] = turn(keys[pl.ds(at, WINDOW), :])
                values_turned[pl.ds(at, WINDOW), :] = turn(values[pl.ds(at, WINDOW), :])

        row = place(t)
        lowest = jnp.where((sp == 0) & (t == chunks - 1), WINDOW, 0)
        highest = jnp.where((sp == sp_count - 1) & (t == chunks - 2), 2 * WINDOW, 3 * WINDOW)
        att[...] = attend(
            row, row, q_ref, (keys, keys_turned, values, values_turned), sink_ref, lowest, highest
        )

        def part(block, half):
            at = pl.ds(pl.multiple_of(block * 512 + 256 * half, 256), 256)
            return jnp.dot(att[...], proj_ref[:, at], preferred_element_type=F32).astype(BF16)

        scatter.first(t, part)

    def mix(s):
        half0, half1 = scatter.last(s)
        mixed[s, :, :256] = half0
        mixed[s, :, 256:] = half1
        sums.give(s, half0, half1)

    def first_rows(s):
        scale = lax.rsqrt(sums.take(s) / 2048.0 + EPS)
        res = res_ref[pl.ds(place(s), WINDOW), :].astype(F32)
        rows[me, s] = (res + mixed[s] * scale * gain_mix).astype(BF16)
        gather(s, 0).start()
        gather(s, 1).start()

    def relay(s):
        for m in (0, 1):
            arrived(s, m)
            gather(s, m + 2).start()

    def feed(u):
        for k in range(2):
            squared = jnp.zeros((WINDOW, 1), F32)
            for b in range(4):
                x = rows[b, 2 * u + k].astype(F32)
                squared += jnp.sum(x * x, axis=1, keepdims=True)
            scale = lax.rsqrt(squared / 2048.0 + EPS)
            for b in range(4):
                x = rows[b, 2 * u + k].astype(F32)
                normed[WINDOW * k : WINDOW * k + WINDOW, 512 * b : 512 * b + 512] = (
                    x * scale * gain_pre_ref[:, 512 * b : 512 * b + 512]
                ).astype(BF16)

        def tile(j, carry):
            both = jnp.dot(
                normed[...], whole[:, pl.ds(pl.multiple_of(j * 256, 256), 256)],
                preferred_element_type=F32,
            )
            gate, up = both[:, :128], both[:, 128:]
            hidden[:, pl.ds(pl.multiple_of(j * 128, 128), 128)] = (
                gate / (1.0 + jnp.exp(-gate)) * up
            ).astype(BF16)
            return carry

        lax.fori_loop(0, tiles, tile, 0)

        def part(block, half):
            at = pl.ds(pl.multiple_of(block * 512 + 256 * half, 256), 256)
            return lax.dot_general(
                hidden[...], whole[at, inner : inner + units], NT, preferred_element_type=F32
            ).astype(BF16)

        f_scatter.first(u, part)

    def feed_sum(u):
        half0, half1 = f_scatter.last(u)
        f_total[u, :, :256] = half0
        f_total[u, :, 256:] = half1
        f_sums.give(u, half0, half1)

    def finish(u):
        scale = lax.rsqrt(f_sums.take(u) / 2048.0 + EPS)
        for k in range(2):
            part = pl.ds(WINDOW * k, WINDOW)
            out_ref[pl.ds(place(2 * u + k), WINDOW), :] = (
                rows[me, 2 * u + k].astype(F32)
                + 0.5 * (f_total[u, part, :] * scale[WINDOW * k : WINDOW * k + WINDOW] * gain_post)
            ).astype(BF16)

    def step(t, carry):
        def when(lag, fn):
            @pl.when((t >= lag) & (t < chunks + lag))
            def _():
                fn(t - lag)

        def when_fed(lag, fn):
            begin = FEED_AT + lag

            @pl.when((t >= begin) & (t < begin + chunks) & (lax.rem(t - begin + chunks, 2) == 0))
            def _():
                fn(lax.div(t - begin, 2))

        when(0, attention)
        when(1, scatter.second)
        when_fed(1, f_scatter.second)
        when(2, mix)
        when_fed(2, feed_sum)
        when(3, first_rows)
        when(4, relay)
        when_fed(3, finish)

        @pl.when((t >= 5) & (t < chunks + 5))
        def _():
            arrived(t - 5, 2)
            arrived(t - 5, 3)

        for n in range(1, 8):
            @pl.when(t == n)
            def _():
                weights.step(n)

        when_fed(0, feed)
        return carry

    lax.fori_loop(0, FEED_AT + chunks + 2, step, 0)

    for n in range(4):
        halo(n).wait_send()
    weights.drain()

    def drain(slot, carry):
        scatter.drain(slot)
        sums.drain(slot)
        for m in range(4):
            gather(slot, m).wait_send()
        return carry

    lax.fori_loop(0, chunks, drain, 0)

    def f_drain(slot, carry):
        f_scatter.drain(slot)
        f_sums.drain(slot)
        return carry

    lax.fori_loop(0, half_chunks, f_drain, 0)


def sems(*shapes):
    return [pltpu.SemaphoreType.DMA(s) for s in shapes]


def body(
    residual, rotated_query_rows, rotated_key_rows, value_matrix_rows, head_sink_logit,
    out_proj, gain_mix, gain_pre, gain_post, gate_proj, up_proj, down_proj,
):
    length = residual.shape[0]
    chunks = length // WINDOW
    half = chunks // 2
    units = gate_proj.shape[1]
    sp_count = lax.axis_size("sp")
    full = sp_count * gate_proj.shape[0]
    big = 2 * WINDOW
    vmem = pl.BlockSpec(memory_space=pltpu.VMEM)
    smem = pl.BlockSpec(memory_space=pltpu.SMEM)
    hbm = pl.BlockSpec(memory_space=pl.ANY)
    loaded = (
        residual, rotated_query_rows, rotated_key_rows, value_matrix_rows, out_proj,
        gate_proj, up_proj, down_proj,
    )
    return pl.pallas_call(
        functools.partial(layer_kernel, chunks, sp_count),
        out_shape=jax.ShapeDtypeStruct(residual.shape, BF16),
        in_specs=[hbm] * 4 + [smem, hbm] + [vmem] * 3 + [hbm] * 3,
        out_specs=vmem,
        scratch_shapes=[pltpu.VMEM(a.shape, BF16) for a in loaded]
        + [pltpu.VMEM((full, 3 * units), BF16)]
        + [pltpu.VMEM((length + big, 128), BF16)] * 4
        + [
            pltpu.VMEM((WINDOW, 384), BF16),
            pltpu.VMEM((chunks, 6, WINDOW, 256), BF16),
            pltpu.VMEM((chunks, 6, WINDOW, 256), BF16),
            pltpu.VMEM((chunks, WINDOW, 512), BF16),
            pltpu.VMEM((chunks, WINDOW, 512), F32),
            pltpu.VMEM((chunks, 8, 128), F32),
            pltpu.VMEM((chunks, 3, 8, 128), F32),
            pltpu.VMEM((4, chunks, WINDOW, 512), BF16),
            pltpu.VMEM((big, full), BF16),
            pltpu.VMEM((big, units), BF16),
            pltpu.VMEM((half, 6, big, 256), BF16),
            pltpu.VMEM((half, 6, big, 256), BF16),
            pltpu.VMEM((half, big, 512), BF16),
            pltpu.VMEM((half, big, 512), F32),
            pltpu.VMEM((half, 16, 128), F32),
            pltpu.VMEM((half, 3, 16, 128), F32),
        ]
        + sems((8,), (2, 5, 4), (2, 5, 4), (2, 16), (2, 16))
        + sems((4,), (4,), (chunks, 6), (chunks, 6), (chunks, 3), (chunks, 3), (chunks, 4), (chunks, 4))
        + sems((half, 6), (half, 6), (half, 3), (half, 3)),
        compiler_params=pltpu.CompilerParams(
            collective_id=0, has_side_effects=True, vmem_limit_bytes=63 * 2**20
        ),
    )(
        residual, rotated_query_rows, rotated_key_rows, value_matrix_rows, head_sink_logit,
        out_proj, gain_mix[None], gain_pre[None], gain_post[None], gate_proj, up_proj, down_proj,
    )


def solution(mesh):
    placed = (
        P("sp", "tp"), P("sp", "tp"), P("sp", "tp"), P("sp", "tp"), P("tp"), P("tp", None),
        P(), P(), P(), P("sp", "tp"), P("sp", "tp"), P("tp", "sp"),
    )
    return jax.shard_map(body, mesh=mesh, in_specs=placed, out_specs=P("sp", "tp"), check_vma=False)
```

time: 165 us -> 152 us (0.921)
  between operations: 13.5 us -> 0.01 us
  Pallas kernels: 138 us -> 147 us
  local copies, waits for them, and re-layouts: 11.2 us -> 4.09 us
  other arithmetic: 2.02 us -> 0 us
    pallas_call x2 -> x1, Pallas kernels: 138 us -> 147 us  [body(): pl.pallas_call(functools.partial(layer_kernel, chunks, sp_count), out_sha...]
    another operation x3 -> x0, local copies, waits for them, and re-layouts: 3.22 us -> none  [body(): jnp.stack([gate_proj.reshape(depth, units // 128, 128), up_proj.reshape(d...]
    unnamed x17 -> x2, local copies, waits for them, and re-layouts: 6.17 us -> 4.09 us
    concatenate x1 -> x0, other arithmetic: 1.92 us -> none  [body(): jnp.concatenate([both, down_proj.T], axis=1)]
    reshape x1 -> x0, local copies, waits for them, and re-layouts: 1.86 us -> none  [body(): both = jnp.stack([gate_proj.reshape(depth, units // 128, 128), up_proj.re...]
  transfers between devices with their start and end apart: 1 -> 0, of which waited for: 0 -> 0; matrix products, arithmetic and copies ran while one was open for 0% -> 0% of each run, Pallas kernels for 50% -> 0%
where the time goes in v2:
time: 152 us; the launch traced here: 151 us
  Pallas kernels  147 us (97%)
  local copies, waits for them, and re-layouts  4.09 us (3%)
    pallas_call x1, Pallas kernels, body(): pl.pallas_call(functools.partial(layer_kernel, chunks, sp_count), out_sha...  147 us
    unnamed x2, local copies, waits for them, and re-layouts  4.09 us

profile of v2, /device:TPU:0, one launch (start us, length us, event | category | flops | bytes accessed | tf_op | source)
XLA Modules:
  0.0 151.3 jit_solution(5886357252462400002)
XLA Ops:
  0.0 1.8 %copy.13.down_hbm = bf16[1408,64]{1,0:T(8,128)(2,1)} copy(bf16[1408,64]{0,1:T(8,128)(2,1)} %param.23) | data formatting | bytes 360448 | tf_op args[11]
  1.8 147.2 %shard_map.118 = bf16[1024,512]{1,0:T(8,128)(2,1)} custom-call(bf16[1024,512]{1,0:T(8,128)(2,1)} %res_hbm.1, bf16[1024,384]{1,0:T(8,128)(2,1)} %q_hbm.1, bf16[1024,128]{1,0:T(8,128)(2,1)} %k_hbm.1, bf16[1024,128]{1,0:T(8,128)(2,1)} %v_hbm.1, f32[6]{0:T(128)} %sink_ref.1, bf16[384,2048]{1,0:T(8,128)(2,1)} %proj_hbm.1, f32[1,2048]{1,0:T(1,128)} %bitcast.3, ...), custom_call_target="tpu_custom_call" | custom-call | tf_op jit(solution)/shard_map/pallas_call | solution.py:535
  149.1 2.3 %copy.15 = bf16[1024,512]{1,0:T(8,128)(2,1)} copy(bf16[1024,512]{1,0:T(8,128)(2,1)} %shard_map.118) | data formatting | bytes 2097152

commit v3 on v2

--- a/solution.py
+++ b/solution.py
@@ -9,7 +9,7 @@
 
 WINDOW = 128
 EPS = 1e-06
-FEED_AT = 8
+FEED, SECOND, SUM, FINISH = (8, 9, 10, 12), (9, 10, 11, 13), (10, 11, 12, 14), (11, 12, 13, 15)
 MESH = pl.DeviceIdType.MESH
 F32 = jnp.float32
 BF16 = jnp.bfloat16
@@ -43,12 +43,12 @@
 
     def first(self, slot, part):
         self.sent[slot, 0] = part(self.far, 0)
+        self.sent[slot, 1] = part(self.far, 1)
         self.copy(slot, 0).start()
-        self.sent[slot, 1] = part(self.far, 1)
         self.copy(slot, 1).start()
         self.sent[slot, 2] = part(self.right, 1)
+        self.sent[slot, 3] = part(self.left, 0)
         self.copy(slot, 2).start()
-        self.sent[slot, 3] = part(self.left, 0)
         self.copy(slot, 3).start()
         self.sent[slot, 4] = part(self.right, 0)
         self.sent[slot, 5] = part(self.left, 1)
@@ -308,7 +308,7 @@
         whole[shard, 256 * j : 256 * j + 128] = gate_ref[:, 128 * j : 128 * j + 128]
         whole[shard, 256 * j + 128 : 256 * j + 256] = up_ref[:, 128 * j : 128 * j + 128]
         whole[shard, inner + 128 * j : inner + 128 * j + 128] = (
-            down_ref[128 * j : 128 * j + 128, :].astype(F32).T.astype(BF16)
+            down_ref[:, 128 * j : 128 * j + 128]
         )
     for load in loads[3:5]:
         load.wait()
@@ -416,18 +416,12 @@
                     x * scale * gain_pre_ref[:, 512 * b : 512 * b + 512]
                 ).astype(BF16)
 
-        def tile(j, carry):
+        for j in range(tiles):
             both = jnp.dot(
-                normed[...], whole[:, pl.ds(pl.multiple_of(j * 256, 256), 256)],
-                preferred_element_type=F32,
+                normed[...], whole[:, 256 * j : 256 * j + 256], preferred_element_type=F32
             )
             gate, up = both[:, :128], both[:, 128:]
-            hidden[:, pl.ds(pl.multiple_of(j * 128, 128), 128)] = (
-                gate / (1.0 + jnp.exp(-gate)) * up
-            ).astype(BF16)
-            return carry
-
-        lax.fori_loop(0, tiles, tile, 0)
+            hidden[:, 128 * j : 128 * j + 128] = (gate / (1.0 + jnp.exp(-gate)) * up).astype(BF16)
 
         def part(block, half):
             at = pl.ds(pl.multiple_of(block * 512 + 256 * half, 256), 256)
@@ -458,21 +452,20 @@
             def _():
                 fn(t - lag)
 
-        def when_fed(lag, fn):
-            begin = FEED_AT + lag
-
-            @pl.when((t >= begin) & (t < begin + chunks) & (lax.rem(t - begin + chunks, 2) == 0))
+        def when_fed(times, fn):
+            now, index = t == times[0], 0
+            for n in times[1:]:
+                now, index = now | (t == n), index + (t >= n).astype(jnp.int32)
+
+            @pl.when(now)
             def _():
-                fn(lax.div(t - begin, 2))
+                fn(index)
 
         when(0, attention)
         when(1, scatter.second)
-        when_fed(1, f_scatter.second)
         when(2, mix)
-        when_fed(2, feed_sum)
         when(3, first_rows)
         when(4, relay)
-        when_fed(3, finish)
 
         @pl.when((t >= 5) & (t < chunks + 5))
         def _():
@@ -484,10 +477,13 @@
             def _():
                 weights.step(n)
 
-        when_fed(0, feed)
+        when_fed(FEED, feed)
+        when_fed(SECOND, f_scatter.second)
+        when_fed(SUM, feed_sum)
+        when_fed(FINISH, finish)
         return carry
 
-    lax.fori_loop(0, FEED_AT + chunks + 2, step, 0)
+    lax.fori_loop(0, FINISH[-1] + 1, step, 0)
 
     for n in range(4):
         halo(n).wait_send()
@@ -530,7 +526,7 @@
     hbm = pl.BlockSpec(memory_space=pl.ANY)
     loaded = (
         residual, rotated_query_rows, rotated_key_rows, value_matrix_rows, out_proj,
-        gate_proj, up_proj, down_proj,
+        gate_proj, up_proj, down_proj.T,
     )
     return pl.pallas_call(
         functools.partial(layer_kernel, chunks, sp_count),
@@ -562,11 +558,11 @@
         + sems((4,), (4,), (chunks, 6), (chunks, 6), (chunks, 3), (chunks, 3), (chunks, 4), (chunks, 4))
         + sems((half, 6), (half, 6), (half, 3), (half, 3)),
         compiler_params=pltpu.CompilerParams(
-            collective_id=0, has_side_effects=True, vmem_limit_bytes=63 * 2**20
+            collective_id=0, has_side_effects=True, vmem_limit_bytes=54 * 2**20
         ),
     )(
         residual, rotated_query_rows, rotated_key_rows, value_matrix_rows, head_sink_logit,
-        out_proj, gain_mix[None], gain_pre[None], gain_post[None], gate_proj, up_proj, down_proj,
+        out_proj, gain_mix[None], gain_pre[None], gain_post[None], *loaded[5:],
     )
 
 

time: 152 us -> 133 us (0.88)
  Pallas kernels: 147 us -> 130 us
  local copies, waits for them, and re-layouts: 4.09 us -> 2.26 us
    pallas_call x1, Pallas kernels: 147 us -> 130 us  [body(): pl.pallas_call(functools.partial(layer_kernel, chunks, sp_count), out_sha...]
    unnamed x2 -> x1, local copies, waits for them, and re-layouts: 4.09 us -> 2.26 us
where the time goes in v3:
time: 133 us
  Pallas kernels  130 us (98%)
  local copies, waits for them, and re-layouts  2.26 us (2%)
    pallas_call x1, Pallas kernels, body(): pl.pallas_call(functools.partial(layer_kernel, chunks, sp_count), out_sha...  130 us

profile of v3, /device:TPU:0, one launch (start us, length us, event | category | flops | bytes accessed | tf_op | source)
XLA Modules:
  0.0 132.6 jit_solution(13340324262592708195)
XLA Ops:
  0.0 130.4 %shard_map.118 = bf16[1024,512]{1,0:T(8,128)(2,1)} custom-call(bf16[1024,512]{1,0:T(8,128)(2,1)} %res_hbm.1, bf16[1024,384]{1,0:T(8,128)(2,1)} %q_hbm.1, bf16[1024,128]{1,0:T(8,128)(2,1)} %k_hbm.1, bf16[1024,128]{1,0:T(8,128)(2,1)} %v_hbm.1, f32[6]{0:T(128)} %sink_ref.1, bf16[384,2048]{1,0:T(8,128)(2,1)} %proj_hbm.1, f32[1,2048]{1,0:T(1,128)} %bitcast.5, ...), custom_call_target="tpu_custom_call" | custom-call | tf_op jit(solution)/shard_map/pallas_call | solution.py:531
  130.4 2.3 %copy.14 = bf16[1024,512]{1,0:T(8,128)(2,1)} copy(bf16[1024,512]{1,0:T(8,128)(2,1)} %shard_map.118) | data formatting | bytes 2097152

commit v4 on v3

--- a/solution.py
+++ b/solution.py
@@ -10,6 +10,7 @@
 WINDOW = 128
 EPS = 1e-06
 FEED, SECOND, SUM, FINISH = (8, 9, 10, 12), (9, 10, 11, 13), (10, 11, 12, 14), (11, 12, 13, 15)
+DRAIN = 7
 MESH = pl.DeviceIdType.MESH
 F32 = jnp.float32
 BF16 = jnp.bfloat16
@@ -38,8 +39,12 @@
         to = self.right if m % 2 == 0 else self.left
         return tp_copy(
             self.sent.at[slot, m], self.got.at[slot, m],
-            self.send.at[slot, m], self.recv.at[slot, m], to,
-        )
+            self.send.at[slot], self.recv.at[slot, 0 if m < 2 else 1], to,
+        )
+
+    def arrived(self, slot, group):
+        ref = self.got.at[slot, pl.ds(2 * group, 2 + 2 * group)]
+        tp_copy(ref, ref, self.send.at[slot], self.recv.at[slot, group], self.right).wait_recv()
 
     def first(self, slot, part):
         self.sent[slot, 0] = part(self.far, 0)
@@ -56,15 +61,14 @@
         self.own[slot, :, 256:] = part(self.me, 1)
 
     def second(self, slot):
+        self.arrived(slot, 0)
         for k in (0, 1):
-            self.copy(slot, k).wait_recv()
             total = self.sent[slot, 4 + k].astype(F32) + self.got[slot, k].astype(F32)
             self.sent[slot, 4 + k] = total.astype(BF16)
             self.copy(slot, 4 + k).start()
 
     def last(self, slot):
-        for m in (2, 3, 4, 5):
-            self.copy(slot, m).wait_recv()
+        self.arrived(slot, 1)
         half0 = (
             self.own[slot, :, :256].astype(F32)
             + self.got[slot, 4].astype(F32)
@@ -78,8 +82,8 @@
         return half0, half1
 
     def drain(self, slot):
-        for m in range(6):
-            self.copy(slot, m).wait_send()
+        ref = self.sent.at[slot]
+        tp_copy(ref, ref, self.send.at[slot], self.recv.at[slot, 0], self.right).wait_send()
 
 
 class Squares:
@@ -91,8 +95,12 @@
         for m, to in enumerate((self.right, self.left, self.far)):
             yield tp_copy(
                 self.mine.at[slot], self.got.at[slot, m],
-                self.send.at[slot, m], self.recv.at[slot, m], to,
+                self.send.at[slot], self.recv.at[slot], to,
             )
+
+    def all(self, slot):
+        ref = self.got.at[slot]
+        return tp_copy(ref, ref, self.send.at[slot], self.recv.at[slot], self.right)
 
     def give(self, slot, half0, half1):
         total = jnp.sum(half0 * half0, axis=1, keepdims=True) + jnp.sum(
@@ -105,8 +113,7 @@
             copy.start()
 
     def take(self, slot):
-        for copy in self.copies(slot):
-            copy.wait_recv()
+        self.all(slot).wait_recv()
         total = self.mine[slot] + self.got[slot, 0] + self.got[slot, 1] + self.got[slot, 2]
         columns = [
             jnp.broadcast_to(total[8 * g : 8 * g + 1], (128, 128)).T[:, :1]
@@ -115,8 +122,7 @@
         return columns[0] if len(columns) == 1 else jnp.concatenate(columns, axis=0)
 
     def drain(self, slot):
-        for copy in self.copies(slot):
-            copy.wait_send()
+        self.all(slot).wait_send()
 
 
 def attend(row, first_key, q_ref, kv, sink_ref, lowest, highest):
@@ -182,22 +188,29 @@
     def at(self, stage, k):
         return (k, 0) if stage == 0 else (self.across[stage - 1], k)
 
-    def copy(self, way, stage, m, incoming=False):
-        offset = ((3, 1, 2, 2) if incoming else (0, 0, 3, 1))[m]
+    def copy(self, way, stage, m):
+        offset = (0, 0, 3, 1)[m]
         ref = self.rows(way, *self.at(stage, offset), self.core, None if m < 2 else m - 2)
         to = self.device(way, *((1 if m % 2 == 0 else 3, 0) if stage == 0 else (0, 1 if m % 2 == 0 else 3)), self.core)
         return pltpu.make_async_remote_copy(
             src_ref=ref, dst_ref=ref,
-            send_sem=self.send.at[way, stage, m], recv_sem=self.recv.at[way, stage, m],
+            send_sem=self.send.at[way, stage], recv_sem=self.recv.at[way, stage, 0 if m < 2 else 1],
             device_id={"sp": to}, device_id_type=MESH,
         )
 
-    def over(self, way, a, b, incoming=False):
-        ref = self.rows(way, a, b, 1 - self.core if incoming else self.core)
+    def over(self, way, a, b):
+        ref = self.rows(way, a, b, self.core)
         return pltpu.make_async_remote_copy(
             src_ref=ref, dst_ref=ref,
-            send_sem=self.core_send.at[way, 4 * a + b], recv_sem=self.core_recv.at[way, 4 * a + b],
+            send_sem=self.core_send.at[way, a], recv_sem=self.core_recv.at[way, a],
             device_id={"sp": self.device(way, 0, 0, 1 - self.core)}, device_id_type=MESH,
+        )
+
+    def some(self, count, send, recv):
+        ref = self.whole.at[pl.ds(0, count), :]
+        return pltpu.make_async_remote_copy(
+            src_ref=ref, dst_ref=ref, send_sem=send, recv_sem=recv,
+            device_id={"sp": self.device(0, 0, 0, 1 - self.core)}, device_id_type=MESH,
         )
 
     def open(self, way, stage):
@@ -205,17 +218,16 @@
         self.copy(way, stage, 1).start()
 
     def relay(self, way, stage):
-        for m in (0, 1):
-            self.copy(way, stage, m, True).wait_recv()
-            self.copy(way, stage, m + 2).start()
+        self.some(64, self.send.at[way, stage], self.recv.at[way, stage, 0]).wait_recv()
+        self.copy(way, stage, 2).start()
+        self.copy(way, stage, 3).start()
 
     def share(self, way, stage, ks):
         for k in ks:
             self.over(way, *self.at(stage, k)).start()
 
     def close(self, way, stage):
-        for m in (2, 3):
-            self.copy(way, stage, m, True).wait_recv()
+        self.some(32, self.send.at[way, stage], self.recv.at[way, stage, 1]).wait_recv()
         self.share(way, stage, (2,))
 
     def step(self, n):
@@ -251,29 +263,26 @@
                     self.close(way, stage)
             elif n == 7:
                 for a in range(4):
-                    for b in range(4):
-                        self.over(way, a, b, True).wait_recv()
+                    self.some(128, self.core_send.at[way, a], self.core_recv.at[way, a]).wait_recv()
 
     def drain(self):
         for way in (0, 1):
             for stage in range(5):
-                for m in range(4):
-                    self.copy(way, stage, m).wait_send()
+                self.some(96, self.send.at[way, stage], self.recv.at[way, stage, 0]).wait_send()
             for a in range(4):
-                for b in range(4):
-                    self.over(way, a, b).wait_send()
+                self.some(128, self.core_send.at[way, a], self.core_recv.at[way, a]).wait_send()
 
 
 def layer_kernel(
     chunks, sp_count,
     res_hbm, q_hbm, k_hbm, v_hbm, sink_ref, proj_hbm, gain_mix_ref, gain_pre_ref, gain_post_ref,
     gate_hbm, up_hbm, down_hbm,
-    out_ref,
-    res_ref, q_ref, k_ref, v_ref, proj_ref, gate_ref, up_ref, down_ref,
+    out_hbm,
+    done, res_ref, q_ref, k_ref, v_ref, proj_ref, gate_ref, up_ref, down_ref,
     whole, keys, keys_turned, values, values_turned, att,
     sent, got, own, mixed, mine, squares, rows,
     normed, hidden, f_sent, f_got, f_own, f_total, f_mine, f_squares,
-    load_sem, w_send, w_recv, core_send, core_recv,
+    out_sem, load_sem, w_send, w_recv, core_send, core_recv,
     halo_send, halo_recv, rs_send, rs_recv, sq_send, sq_recv, ag_send, ag_recv,
     f_rs_send, f_rs_recv, f_sq_send, f_sq_recv,
 ):
@@ -321,10 +330,12 @@
         else:
             src, dst, to = mine_ref.at[pl.ds(0, WINDOW)], both.at[pl.ds(length + WINDOW, WINDOW)], before
         return pltpu.make_async_remote_copy(
-            src_ref=src, dst_ref=dst, send_sem=halo_send.at[n], recv_sem=halo_recv.at[n],
+            src_ref=src, dst_ref=dst, send_sem=halo_send, recv_sem=halo_recv,
             device_id={"sp": to}, device_id_type=MESH,
         )
 
+    halos = keys.at[pl.ds(0, 4 * WINDOW)]
+    halos = tp_copy(halos, halos, halo_send, halo_recv, right)
     for n in range(4):
         halo(n).start()
     weights.step(0)
@@ -353,21 +364,16 @@
             (left, right, pl.ds(0, 256)), (right, left, pl.ds(256, 256)),
         )[m]
         ref = rows.at[owner, slot, :, part]
-        return tp_copy(ref, ref, ag_send.at[slot, m], ag_recv.at[slot, m], to)
-
-    def arrived(slot, m):
-        owner, part = (
-            (left, pl.ds(0, 512)), (right, pl.ds(0, 512)),
-            (far, pl.ds(0, 256)), (far, pl.ds(256, 256)),
-        )[m]
-        ref = rows.at[owner, slot, :, part]
-        tp_copy(ref, ref, ag_send.at[slot, m], ag_recv.at[slot, m], right).wait_recv()
+        return tp_copy(ref, ref, ag_send.at[slot], ag_recv.at[slot, 0 if m < 2 else 1], to)
+
+    def gathers(slot, blocks, group):
+        ref = rows.at[pl.ds(0, blocks), slot]
+        return tp_copy(ref, ref, ag_send.at[slot], ag_recv.at[slot, group], right)
 
     def attention(t):
         @pl.when(t == chunks - 2)
         def _():
-            for n in range(4):
-                halo(n).wait_recv()
+            halos.wait_recv()
             for at in (0, length + WINDOW):
                 keys_turned[pl.ds(at, WINDOW), :] = turn(keys[pl.ds(at, WINDOW), :])
                 values_turned[pl.ds(at, WINDOW), :] = turn(values[pl.ds(at, WINDOW), :])
@@ -399,9 +405,9 @@
         gather(s, 1).start()
 
     def relay(s):
-        for m in (0, 1):
-            arrived(s, m)
-            gather(s, m + 2).start()
+        gathers(s, 2, 0).wait_recv()
+        gather(s, 2).start()
+        gather(s, 3).start()
 
     def feed(u):
         for k in range(2):
@@ -441,10 +447,25 @@
         scale = lax.rsqrt(f_sums.take(u) / 2048.0 + EPS)
         for k in range(2):
             part = pl.ds(WINDOW * k, WINDOW)
-            out_ref[pl.ds(place(2 * u + k), WINDOW), :] = (
+            at = pl.ds(place(2 * u + k), WINDOW)
+            done[at, :] = (
                 rows[me, 2 * u + k].astype(F32)
                 + 0.5 * (f_total[u, part, :] * scale[WINDOW * k : WINDOW * k + WINDOW] * gain_post)
             ).astype(BF16)
+            result(2 * u + k).start()
+
+    def result(slot):
+        at = pl.ds(place(slot), WINDOW)
+        return pltpu.make_async_copy(done.at[at, :], out_hbm.at[at, :], out_sem)
+
+    def drain(slot):
+        scatter.drain(slot)
+        sums.drain(slot)
+        gathers(slot, 3, 0).wait_send()
+
+    def f_drain(u):
+        f_scatter.drain(u)
+        f_sums.drain(u)
 
     def step(t, carry):
         def when(lag, fn):
@@ -469,8 +490,7 @@
 
         @pl.when((t >= 5) & (t < chunks + 5))
         def _():
-            arrived(t - 5, 2)
-            arrived(t - 5, 3)
+            gathers(t - 5, 1, 1).wait_recv()
 
         for n in range(1, 8):
             @pl.when(t == n)
@@ -481,29 +501,19 @@
         when_fed(SECOND, f_scatter.second)
         when_fed(SUM, feed_sum)
         when_fed(FINISH, finish)
+        when(DRAIN, drain)
+
+        @pl.when(t == DRAIN)
+        def _():
+            halos.wait_send()
+            weights.drain()
+
+        when_fed(FINISH[1:], f_drain)
         return carry
 
     lax.fori_loop(0, FINISH[-1] + 1, step, 0)
-
-    for n in range(4):
-        halo(n).wait_send()
-    weights.drain()
-
-    def drain(slot, carry):
-        scatter.drain(slot)
-        sums.drain(slot)
-        for m in range(4):
-            gather(slot, m).wait_send()
-        return carry
-
-    lax.fori_loop(0, chunks, drain, 0)
-
-    def f_drain(slot, carry):
-        f_scatter.drain(slot)
-        f_sums.drain(slot)
-        return carry
-
-    lax.fori_loop(0, half_chunks, f_drain, 0)
+    f_drain(half_chunks - 1)
+    pltpu.make_async_copy(done, out_hbm, out_sem).wait()
 
 
 def sems(*shapes):
@@ -532,8 +542,9 @@
         functools.partial(layer_kernel, chunks, sp_count),
         out_shape=jax.ShapeDtypeStruct(residual.shape, BF16),
         in_specs=[hbm] * 4 + [smem, hbm] + [vmem] * 3 + [hbm] * 3,
-        out_specs=vmem,
-        scratch_shapes=[pltpu.VMEM(a.shape, BF16) for a in loaded]
+        out_specs=hbm,
+        scratch_shapes=[pltpu.VMEM(residual.shape, BF16)]
+        + [pltpu.VMEM(a.shape, BF16) for a in loaded]
         + [pltpu.VMEM((full, 3 * units), BF16)]
         + [pltpu.VMEM((length + big, 128), BF16)] * 4
         + [
@@ -554,9 +565,11 @@
             pltpu.VMEM((half, 16, 128), F32),
             pltpu.VMEM((half, 3, 16, 128), F32),
         ]
-        + sems((8,), (2, 5, 4), (2, 5, 4), (2, 16), (2, 16))
-        + sems((4,), (4,), (chunks, 6), (chunks, 6), (chunks, 3), (chunks, 3), (chunks, 4), (chunks, 4))
-        + sems((half, 6), (half, 6), (half, 3), (half, 3)),
+        + [pltpu.SemaphoreType.DMA]
+        + sems((8,), (2, 5), (2, 5, 2), (2, 4), (2, 4))
+        + [pltpu.SemaphoreType.DMA] * 2
+        + sems((chunks,), (chunks, 2), (chunks,), (chunks,), (chunks,), (chunks, 2))
+        + sems((half,), (half, 2), (half,), (half,)),
         compiler_params=pltpu.CompilerParams(
             collective_id=0, has_side_effects=True, vmem_limit_bytes=54 * 2**20
         ),

time: 133 us -> 130 us (0.977)
  Pallas kernels: 130 us -> 128 us
    pallas_call x1, Pallas kernels: 130 us -> 128 us  [body(): pl.pallas_call(functools.partial(layer_kernel, chunks, sp_count), out_sha...]
where the time goes in v4:
time: 130 us
  Pallas kernels  128 us (98%)
  local copies, waits for them, and re-layouts  2.26 us (2%)
    pallas_call x1, Pallas kernels, body(): pl.pallas_call(functools.partial(layer_kernel, chunks, sp_count), out_sha...  128 us

profile of v4, /device:TPU:0, one launch (start us, length us, event | category | flops | bytes accessed | tf_op | source)
XLA Modules:
  0.0 130.0 jit_solution(11016834195901291062)
XLA Ops:
  0.0 127.7 %shard_map.118 = bf16[1024,512]{1,0:T(8,128)(2,1)} custom-call(bf16[1024,512]{1,0:T(8,128)(2,1)} %res_hbm.1, bf16[1024,384]{1,0:T(8,128)(2,1)} %q_hbm.1, bf16[1024,128]{1,0:T(8,128)(2,1)} %k_hbm.1, bf16[1024,128]{1,0:T(8,128)(2,1)} %v_hbm.1, f32[6]{0:T(128)} %sink_ref.1, bf16[384,2048]{1,0:T(8,128)(2,1)} %proj_hbm.1, f32[1,2048]{1,0:T(1,128)} %bitcast.5, ...), custom_call_target="tpu_custom_call" | custom-call | tf_op jit(solution)/shard_map/pallas_call | solution.py:541
  127.7 2.3 %copy.14 = bf16[1024,512]{1,0:T(8,128)(2,1)} copy(bf16[1024,512]{1,0:T(8,128)(2,1)} %shard_map.118) | data formatting | bytes 2097152

commit v5 on v4

--- a/solution.py
+++ b/solution.py
@@ -9,8 +9,11 @@
 
 WINDOW = 128
 EPS = 1e-06
-FEED, SECOND, SUM, FINISH = (8, 9, 10, 12), (9, 10, 11, 13), (10, 11, 12, 14), (11, 12, 13, 15)
-DRAIN = 7
+MIX = 4
+PROJECTION = (0, 1, 2, 3, 4)
+WEIGHTS = (5, 5, 4, 6, 6, 8, 9, 10, 12), (2, 5, 6, 4, 6, 8, 10, 12, 12)
+FEED, SECOND, SUM, FINISH = (12, 13, 14, 15), (13, 14, 15, 16), (14, 15, 16, 17), (15, 16, 17, 18)
+DRAIN = 9
 MESH = pl.DeviceIdType.MESH
 F32 = jnp.float32
 BF16 = jnp.bfloat16
@@ -123,6 +126,100 @@
 
     def drain(self, slot):
         self.all(slot).wait_send()
+
+
+class Gather:
+    def __init__(self, buffer, send, recv):
+        self.buffer, self.send, self.recv = buffer, send, recv
+        self.me, self.right, self.left, self.far = ring()
+
+    def copy(self, slot, owner, to, group, part):
+        ref = self.buffer.at[owner, slot, part]
+        return tp_copy(ref, ref, self.send.at[slot], self.recv.at[slot, group], to)
+
+    def some(self, slot, blocks, group):
+        ref = self.buffer.at[pl.ds(0, blocks), slot]
+        return tp_copy(ref, ref, self.send.at[slot], self.recv.at[slot, group], self.right)
+
+    def open(self, slot):
+        whole = pl.ds(0, WINDOW)
+        self.copy(slot, self.me, self.right, 0, whole).start()
+        self.copy(slot, self.me, self.left, 0, whole).start()
+
+    def relay(self, slot):
+        self.some(slot, 2, 0).wait_recv()
+        self.copy(slot, self.left, self.right, 1, pl.ds(0, WINDOW // 2)).start()
+        self.copy(slot, self.right, self.left, 1, pl.ds(WINDOW // 2, WINDOW // 2)).start()
+
+    def close(self, slot):
+        self.some(slot, 1, 1).wait_recv()
+
+    def drain(self, slot):
+        self.some(slot, 3, 0).wait_send()
+
+
+class Projection:
+    def __init__(self, taken, source, send, recv):
+        self.taken, self.source, self.send, self.recv = taken, source, send, recv
+        self.me, self.right, self.left, self.far = ring()
+        sp = lax.axis_index("sp")
+        self.core, self.y, self.rest = lax.rem(sp, 2), lax.rem(lax.div(sp, 2), 4), lax.div(sp, 8) * 8
+        self.depth = source.shape[0] // 8
+
+    def columns(self, owner):
+        return pl.ds(pl.multiple_of(owner * 512, 512), 512)
+
+    def eighth(self, dy):
+        start = (2 * lax.rem(self.y + dy, 4) + self.core) * self.depth
+        return pl.ds(pl.multiple_of(start, self.depth), self.depth)
+
+    def to_sp(self, dy, core):
+        return {"sp": self.rest + 2 * lax.rem(self.y + dy, 4) + core}
+
+    def copy(self, src, dst, n, group, to):
+        return pltpu.make_async_remote_copy(
+            src_ref=src, dst_ref=dst, send_sem=self.send.at[n], recv_sem=self.recv.at[group],
+            device_id=to, device_id_type=MESH,
+        )
+
+    def piece(self, dy, n, group, to, part=None):
+        ref = self.taken.at[pl.ds(1, 3), self.eighth(dy), pl.ds(*(part or (0, 512)))]
+        return self.copy(ref, ref, n, group, to)
+
+    def some(self, n, group, pieces):
+        ref = self.taken.at[pl.ds(1, 3), pl.ds(0, pieces * self.depth)]
+        return self.copy(ref, ref, n, group, {"tp": self.right})
+
+    def across(self, dy):
+        self.piece(dy, 2, 3, self.to_sp(0, 1 - self.core)).start()
+
+    def step(self, n):
+        if n == 0:
+            rows = self.eighth(0)
+            for to, k in ((self.right, 3), (self.left, 1), (self.far, 2)):
+                self.copy(
+                    self.source.at[rows, self.columns(to)], self.taken.at[k, rows], 0, 0, {"tp": to}
+                ).start()
+        elif n == 1:
+            self.some(0, 0, 1).wait_recv()
+            self.piece(0, 1, 1, self.to_sp(1, self.core)).start()
+            self.piece(0, 1, 1, self.to_sp(3, self.core)).start()
+            self.across(0)
+        elif n == 2:
+            self.some(1, 1, 2).wait_recv()
+            self.piece(3, 1, 2, self.to_sp(1, self.core), (0, 256)).start()
+            self.piece(1, 1, 2, self.to_sp(3, self.core), (256, 256)).start()
+            self.across(1)
+            self.across(3)
+        elif n == 3:
+            self.some(1, 2, 1).wait_recv()
+            self.across(2)
+        elif n == 4:
+            self.some(2, 3, 4).wait_recv()
+
+    def drain(self):
+        for n, pieces in enumerate((1, 3, 4)):
+            self.some(n, 0, pieces).wait_send()
 
 
 def attend(row, first_key, q_ref, kv, sink_ref, lowest, highest):
@@ -230,40 +327,34 @@
         self.some(32, self.send.at[way, stage], self.recv.at[way, stage, 1]).wait_recv()
         self.share(way, stage, (2,))
 
-    def step(self, n):
-        for way in (0, 1):
-            if n == 0:
-                self.open(way, 0)
-            elif n == 1:
-                self.relay(way, 0)
-        for way in (0, 1):
-            if n == 0:
-                self.open(way, 1)
-                self.over(way, 0, 0).start()
-            elif n == 1:
-                self.open(way, 2)
-                self.open(way, 3)
-                self.share(way, 0, (1, 3))
-            elif n == 2:
-                self.relay(way, 1)
-                self.share(way, 1, (1, 3))
-            elif n == 3:
-                self.close(way, 0)
-                self.open(way, 4)
-            elif n == 4:
-                for stage in (2, 3):
-                    self.relay(way, stage)
-                    self.share(way, stage, (1, 3))
-            elif n == 5:
-                self.close(way, 1)
-                self.relay(way, 4)
-                self.share(way, 4, (1, 3))
-            elif n == 6:
-                for stage in (2, 3, 4):
-                    self.close(way, stage)
-            elif n == 7:
-                for a in range(4):
-                    self.some(128, self.core_send.at[way, a], self.core_recv.at[way, a]).wait_recv()
+    def step(self, way, n):
+        if n == 0:
+            self.relay(way, 0)
+            self.share(way, 0, (1, 3))
+        elif n == 1:
+            self.open(way, 2)
+            self.open(way, 3)
+        elif n == 2:
+            self.relay(way, 1)
+            self.share(way, 1, (1, 3))
+        elif n == 3:
+            self.close(way, 0)
+        elif n == 4:
+            self.open(way, 4)
+        elif n == 5:
+            for stage in (2, 3):
+                self.relay(way, stage)
+                self.share(way, stage, (1, 3))
+        elif n == 6:
+            self.close(way, 1)
+            self.relay(way, 4)
+            self.share(way, 4, (1, 3))
+        elif n == 7:
+            for stage in (2, 3, 4):
+                self.close(way, stage)
+        elif n == 8:
+            for a in range(4):
+                self.some(128, self.core_send.at[way, a], self.core_recv.at[way, a]).wait_recv()
 
     def drain(self):
         for way in (0, 1):
@@ -279,11 +370,11 @@
     gate_hbm, up_hbm, down_hbm,
     out_hbm,
     done, res_ref, q_ref, k_ref, v_ref, proj_ref, gate_ref, up_ref, down_ref,
-    whole, keys, keys_turned, values, values_turned, att,
-    sent, got, own, mixed, mine, squares, rows,
+    whole, keys, keys_turned, values, values_turned, taken, att,
+    mixed, mine, squares, rows,
     normed, hidden, f_sent, f_got, f_own, f_total, f_mine, f_squares,
     out_sem, load_sem, w_send, w_recv, core_send, core_recv,
-    halo_send, halo_recv, rs_send, rs_recv, sq_send, sq_recv, ag_send, ag_recv,
+    halo_send, halo_recv, p_send, p_recv, at_send, at_recv, sq_send, sq_recv, ag_send, ag_recv,
     f_rs_send, f_rs_recv, f_sq_send, f_sq_recv,
 ):
     me, right, left, far = ring()
@@ -298,8 +389,8 @@
     loads = [
         pltpu.make_async_copy(a, b, load_sem.at[n])
         for n, (a, b) in enumerate((
-            (gate_hbm, gate_ref), (up_hbm, up_ref), (down_hbm, down_ref), (k_hbm, k_ref),
-            (v_hbm, v_ref), (q_hbm, q_ref), (proj_hbm, proj_ref), (res_hbm, res_ref),
+            (proj_hbm, proj_ref), (k_hbm, k_ref), (v_hbm, v_ref), (gate_hbm, gate_ref),
+            (up_hbm, up_ref), (down_hbm, down_ref), (q_hbm, q_ref), (res_hbm, res_ref),
         ))
     ]
     for load in loads:
@@ -310,7 +401,7 @@
     others += [{"sp": n} for n in weights.neighbours()]
     for other in others:
         pl.semaphore_signal(barrier, inc=1, device_id=other, device_id_type=MESH)
-    for load in loads[:3]:
+    for load in loads[3:6]:
         load.wait()
     shard = pl.ds(pl.multiple_of(sp * 64, 64), 64)
     for j in range(tiles):
@@ -319,7 +410,7 @@
         whole[shard, inner + 128 * j : inner + 128 * j + 128] = (
             down_ref[:, 128 * j : 128 * j + 128]
         )
-    for load in loads[3:5]:
+    for load in loads[:3]:
         load.wait()
     pl.semaphore_wait(barrier, len(others))
 
@@ -338,16 +429,23 @@
     halos = tp_copy(halos, halos, halo_send, halo_recv, right)
     for n in range(4):
         halo(n).start()
-    weights.step(0)
+    projection = Projection(taken, proj_ref, p_send, p_recv)
+    projection.step(0)
+    weights.open(1, 0)
+    weights.open(0, 1)
+    weights.over(0, 0, 0).start()
+    weights.over(1, 0, 0).start()
     middle = pl.ds(WINDOW, length)
     keys[middle, :] = k_ref[...]
     values[middle, :] = v_ref[...]
     keys_turned[middle, :] = turn(k_ref[...])
     values_turned[middle, :] = turn(v_ref[...])
-    for load in loads[5:]:
+    for load in loads[6:]:
         load.wait()
-
-    scatter = Scatter(sent, got, own, rs_send, rs_recv)
+    taken[0] = proj_ref[:, projection.columns(me)]
+
+    mixing = Gather(att, at_send, at_recv)
+    feeding = Gather(rows, ag_send, ag_recv)
     sums = Squares(mine, squares, sq_send, sq_recv)
     f_scatter = Scatter(f_sent, f_got, f_own, f_rs_send, f_rs_recv)
     f_sums = Squares(f_mine, f_squares, f_sq_send, f_sq_recv)
@@ -357,18 +455,6 @@
 
     def place(slot):
         return pl.multiple_of(lax.rem(slot + 1, chunks) * WINDOW, WINDOW)
-
-    def gather(slot, m):
-        owner, to, part = (
-            (me, right, pl.ds(0, 512)), (me, left, pl.ds(0, 512)),
-            (left, right, pl.ds(0, 256)), (right, left, pl.ds(256, 256)),
-        )[m]
-        ref = rows.at[owner, slot, :, part]
-        return tp_copy(ref, ref, ag_send.at[slot], ag_recv.at[slot, 0 if m < 2 else 1], to)
-
-    def gathers(slot, blocks, group):
-        ref = rows.at[pl.ds(0, blocks), slot]
-        return tp_copy(ref, ref, ag_send.at[slot], ag_recv.at[slot, group], right)
 
     def attention(t):
         @pl.when(t == chunks - 2)
@@ -381,33 +467,24 @@
         row = place(t)
         lowest = jnp.where((sp == 0) & (t == chunks - 1), WINDOW, 0)
         highest = jnp.where((sp == sp_count - 1) & (t == chunks - 2), 2 * WINDOW, 3 * WINDOW)
-        att[...] = attend(
+        att[me, t] = attend(
             row, row, q_ref, (keys, keys_turned, values, values_turned), sink_ref, lowest, highest
         )
-
-        def part(block, half):
-            at = pl.ds(pl.multiple_of(block * 512 + 256 * half, 256), 256)
-            return jnp.dot(att[...], proj_ref[:, at], preferred_element_type=F32).astype(BF16)
-
-        scatter.first(t, part)
+        mixing.open(t)
 
     def mix(s):
-        half0, half1 = scatter.last(s)
-        mixed[s, :, :256] = half0
-        mixed[s, :, 256:] = half1
-        sums.give(s, half0, half1)
+        mixing.close(s)
+        total = jnp.zeros((WINDOW, 512), F32)
+        for k, owner in enumerate((me, right, far, left)):
+            total += jnp.dot(att[owner, s], taken[k], preferred_element_type=F32)
+        mixed[s] = total
+        sums.give(s, total[:, :256], total[:, 256:])
 
     def first_rows(s):
         scale = lax.rsqrt(sums.take(s) / 2048.0 + EPS)
         res = res_ref[pl.ds(place(s), WINDOW), :].astype(F32)
         rows[me, s] = (res + mixed[s] * scale * gain_mix).astype(BF16)
-        gather(s, 0).start()
-        gather(s, 1).start()
-
-    def relay(s):
-        gathers(s, 2, 0).wait_recv()
-        gather(s, 2).start()
-        gather(s, 3).start()
+        feeding.open(s)
 
     def feed(u):
         for k in range(2):
@@ -459,9 +536,9 @@
         return pltpu.make_async_copy(done.at[at, :], out_hbm.at[at, :], out_sem)
 
     def drain(slot):
-        scatter.drain(slot)
+        mixing.drain(slot)
         sums.drain(slot)
-        gathers(slot, 3, 0).wait_send()
+        feeding.drain(slot)
 
     def f_drain(u):
         f_scatter.drain(u)
@@ -483,19 +560,26 @@
                 fn(index)
 
         when(0, attention)
-        when(1, scatter.second)
-        when(2, mix)
-        when(3, first_rows)
-        when(4, relay)
-
-        @pl.when((t >= 5) & (t < chunks + 5))
-        def _():
-            gathers(t - 5, 1, 1).wait_recv()
-
-        for n in range(1, 8):
-            @pl.when(t == n)
+        when(1, mixing.relay)
+
+        for n in range(1, 5):
+            @pl.when(t == PROJECTION[n])
             def _():
-                weights.step(n)
+                projection.step(n)
+                if n == 2:
+                    weights.open(0, 0)
+                    weights.open(1, 1)
+
+        when(MIX, mix)
+        when(MIX + 1, first_rows)
+        when(MIX + 2, feeding.relay)
+        when(MIX + 3, feeding.close)
+
+        for n in range(9):
+            for way in (0, 1):
+                @pl.when(t == WEIGHTS[way][n])
+                def _():
+                    weights.step(way, n)
 
         when_fed(FEED, feed)
         when_fed(SECOND, f_scatter.second)
@@ -503,10 +587,11 @@
         when_fed(FINISH, finish)
         when(DRAIN, drain)
 
-        @pl.when(t == DRAIN)
+        @pl.when(t == SECOND[0])
         def _():
             halos.wait_send()
             weights.drain()
+            projection.drain()
 
         when_fed(FINISH[1:], f_drain)
         return carry
@@ -548,10 +633,8 @@
         + [pltpu.VMEM((full, 3 * units), BF16)]
         + [pltpu.VMEM((length + big, 128), BF16)] * 4
         + [
-            pltpu.VMEM((WINDOW, 384), BF16),
-            pltpu.VMEM((chunks, 6, WINDOW, 256), BF16),
-            pltpu.VMEM((chunks, 6, WINDOW, 256), BF16),
-            pltpu.VMEM((chunks, WINDOW, 512), BF16),
+            pltpu.VMEM((4, out_proj.shape[0], 512), BF16),
+            pltpu.VMEM((4, chunks, WINDOW, 384), BF16),
             pltpu.VMEM((chunks, WINDOW, 512), F32),
             pltpu.VMEM((chunks, 8, 128), F32),
             pltpu.VMEM((chunks, 3, 8, 128), F32),
@@ -568,7 +651,7 @@
         + [pltpu.SemaphoreType.DMA]
         + sems((8,), (2, 5), (2, 5, 2), (2, 4), (2, 4))
         + [pltpu.SemaphoreType.DMA] * 2
-        + sems((chunks,), (chunks, 2), (chunks,), (chunks,), (chunks,), (chunks, 2))
+        + sems((3,), (4,), (chunks,), (chunks, 2), (chunks,), (chunks,), (chunks,), (chunks, 2))
         + sems((half,), (half, 2), (half,), (half,)),
         compiler_params=pltpu.CompilerParams(
             collective_id=0, has_side_effects=True, vmem_limit_bytes=54 * 2**20

time: 130 us -> 124 us (0.954); the launches traced: 130 us -> 122 us
  Pallas kernels: 128 us -> 120 us
    pallas_call x1, Pallas kernels: 128 us -> 120 us  [body(): pl.pallas_call(functools.partial(layer_kernel, chunks, sp_count), out_sha...]
where the time goes in v5:
time: 124 us; the launch traced here: 122 us
  Pallas kernels  120 us (97%)
  local copies, waits for them, and re-layouts  2.26 us (2%)
    pallas_call x1, Pallas kernels, body(): pl.pallas_call(functools.partial(layer_kernel, chunks, sp_count), out_sha...  120 us

profile of v5, /device:TPU:0, one launch (start us, length us, event | category | flops | bytes accessed | tf_op | source)
XLA Modules:
  0.0 122.5 jit_solution(4825098099028604440)
XLA Ops:
  0.0 120.2 %shard_map.118 = bf16[1024,512]{1,0:T(8,128)(2,1)} custom-call(bf16[1024,512]{1,0:T(8,128)(2,1)} %res_hbm.1, bf16[1024,384]{1,0:T(8,128)(2,1)} %q_hbm.1, bf16[1024,128]{1,0:T(8,128)(2,1)} %k_hbm.1, bf16[1024,128]{1,0:T(8,128)(2,1)} %v_hbm.1, f32[6]{0:T(128)} %sink_ref.1, bf16[384,2048]{1,0:T(8,128)(2,1)} %proj_hbm.1, f32[1,2048]{1,0:T(1,128)} %bitcast.5, ...), custom_call_target="tpu_custom_call" | custom-call | tf_op jit(solution)/shard_map/pallas_call | solution.py:626
  120.2 2.3 %copy.14 = bf16[1024,512]{1,0:T(8,128)(2,1)} copy(bf16[1024,512]{1,0:T(8,128)(2,1)} %shard_map.118) | data formatting | bytes 2097152

commit v6 on v5

--- a/solution.py
+++ b/solution.py
@@ -11,8 +11,9 @@
 EPS = 1e-06
 MIX = 4
 PROJECTION = (0, 1, 2, 3, 4)
-WEIGHTS = (5, 5, 4, 6, 6, 8, 9, 10, 12), (2, 5, 6, 4, 6, 8, 10, 12, 12)
-FEED, SECOND, SUM, FINISH = (12, 13, 14, 15), (13, 14, 15, 16), (14, 15, 16, 17), (15, 16, 17, 18)
+WEIGHTS = (2, 2, 4, 4, 4, 7, 8, 9, 11), (2, 2, 6, 4, 4, 8, 9, 10, 11)
+PREPARE, FEED, SECOND = (11, 12, 13, 14), (12, 13, 14, 15), (13, 14, 15, 16)
+SUM, FINISH = (14, 15, 16, 17), (15, 16, 17, 18)
 DRAIN = 9
 MESH = pl.DeviceIdType.MESH
 F32 = jnp.float32
@@ -332,6 +333,8 @@
             self.relay(way, 0)
             self.share(way, 0, (1, 3))
         elif n == 1:
+            if way == 1:
+                self.open(1, 1)
             self.open(way, 2)
             self.open(way, 3)
         elif n == 2:
@@ -401,15 +404,6 @@
     others += [{"sp": n} for n in weights.neighbours()]
     for other in others:
         pl.semaphore_signal(barrier, inc=1, device_id=other, device_id_type=MESH)
-    for load in loads[3:6]:
-        load.wait()
-    shard = pl.ds(pl.multiple_of(sp * 64, 64), 64)
-    for j in range(tiles):
-        whole[shard, 256 * j : 256 * j + 128] = gate_ref[:, 128 * j : 128 * j + 128]
-        whole[shard, 256 * j + 128 : 256 * j + 256] = up_ref[:, 128 * j : 128 * j + 128]
-        whole[shard, inner + 128 * j : inner + 128 * j + 128] = (
-            down_ref[:, 128 * j : 128 * j + 128]
-        )
     for load in loads[:3]:
         load.wait()
     pl.semaphore_wait(barrier, len(others))
@@ -425,21 +419,31 @@
             device_id={"sp": to}, device_id_type=MESH,
         )
 
+    projection = Projection(taken, proj_ref, p_send, p_recv)
+    projection.step(0)
     halos = keys.at[pl.ds(0, 4 * WINDOW)]
     halos = tp_copy(halos, halos, halo_send, halo_recv, right)
     for n in range(4):
         halo(n).start()
-    projection = Projection(taken, proj_ref, p_send, p_recv)
-    projection.step(0)
-    weights.open(1, 0)
-    weights.open(0, 1)
-    weights.over(0, 0, 0).start()
-    weights.over(1, 0, 0).start()
+    for load in loads[3:6]:
+        load.wait()
+    shard = pl.ds(pl.multiple_of(sp * 64, 64), 64)
+    for j in range(tiles):
+        whole[shard, 256 * j : 256 * j + 128] = gate_ref[:, 128 * j : 128 * j + 128]
+        whole[shard, 256 * j + 128 : 256 * j + 256] = up_ref[:, 128 * j : 128 * j + 128]
+        whole[shard, inner + 128 * j : inner + 128 * j + 128] = (
+            down_ref[:, 128 * j : 128 * j + 128]
+        )
     middle = pl.ds(WINDOW, length)
     keys[middle, :] = k_ref[...]
     values[middle, :] = v_ref[...]
     keys_turned[middle, :] = turn(k_ref[...])
     values_turned[middle, :] = turn(v_ref[...])
+    weights.open(0, 0)
+    weights.open(1, 0)
+    weights.open(0, 1)
+    weights.over(0, 0, 0).start()
+    weights.over(1, 0, 0).start()
     for load in loads[6:]:
         load.wait()
     taken[0] = proj_ref[:, projection.columns(me)]
@@ -486,7 +490,7 @@
         rows[me, s] = (res + mixed[s] * scale * gain_mix).astype(BF16)
         feeding.open(s)
 
-    def feed(u):
+    def prepare(u):
         for k in range(2):
             squared = jnp.zeros((WINDOW, 1), F32)
             for b in range(4):
@@ -504,12 +508,14 @@
                 normed[...], whole[:, 256 * j : 256 * j + 256], preferred_element_type=F32
             )
             gate, up = both[:, :128], both[:, 128:]
-            hidden[:, 128 * j : 128 * j + 128] = (gate / (1.0 + jnp.exp(-gate)) * up).astype(BF16)
-
+            hidden[lax.rem(u, 2), :, 128 * j : 128 * j + 128] = (gate / (1.0 + jnp.exp(-gate)) * up).astype(BF16)
+
+    def feed(u):
         def part(block, half):
             at = pl.ds(pl.multiple_of(block * 512 + 256 * half, 256), 256)
             return lax.dot_general(
-                hidden[...], whole[at, inner : inner + units], NT, preferred_element_type=F32
+                hidden[lax.rem(u, 2)], whole[at, inner : inner + units], NT,
+                preferred_element_type=F32,
             ).astype(BF16)
 
         f_scatter.first(u, part)
@@ -566,20 +572,24 @@
             @pl.when(t == PROJECTION[n])
             def _():
                 projection.step(n)
-                if n == 2:
-                    weights.open(0, 0)
-                    weights.open(1, 1)
 
         when(MIX, mix)
         when(MIX + 1, first_rows)
-        when(MIX + 2, feeding.relay)
-        when(MIX + 3, feeding.close)
 
         for n in range(9):
             for way in (0, 1):
                 @pl.when(t == WEIGHTS[way][n])
                 def _():
                     weights.step(way, n)
+
+        when_fed(PREPARE[:3], prepare)
+        when(MIX + 2, feeding.relay)
+        when(MIX + 3, feeding.close)
+
+        @pl.when(t == PREPARE[3])
+        def _():
+            prepare(3)
+
 
         when_fed(FEED, feed)
         when_fed(SECOND, f_scatter.second)
@@ -640,7 +650,7 @@
             pltpu.VMEM((chunks, 3, 8, 128), F32),
             pltpu.VMEM((4, chunks, WINDOW, 512), BF16),
             pltpu.VMEM((big, full), BF16),
-            pltpu.VMEM((big, units), BF16),
+            pltpu.VMEM((2, big, units), BF16),
             pltpu.VMEM((half, 6, big, 256), BF16),
             pltpu.VMEM((half, 6, big, 256), BF16),
             pltpu.VMEM((half, big, 512), BF16),

time: 124 us -> 120 us (0.968)
  Pallas kernels: 120 us -> 117 us
    pallas_call x1, Pallas kernels: 120 us -> 117 us  [body(): pl.pallas_call(functools.partial(layer_kernel, chunks, sp_count), out_sha...]
where the time goes in v6:
time: 120 us
  Pallas kernels  117 us (98%)
  local copies, waits for them, and re-layouts  2.26 us (2%)
    pallas_call x1, Pallas kernels, body(): pl.pallas_call(functools.partial(layer_kernel, chunks, sp_count), out_sha...  117 us

profile of v6, /device:TPU:0, one launch (start us, length us, event | category | flops | bytes accessed | tf_op | source)
XLA Modules:
  0.0 119.7 jit_solution(4975462173847280003)
XLA Ops:
  0.0 117.4 %shard_map.118 = bf16[1024,512]{1,0:T(8,128)(2,1)} custom-call(bf16[1024,512]{1,0:T(8,128)(2,1)} %res_hbm.1, bf16[1024,384]{1,0:T(8,128)(2,1)} %q_hbm.1, bf16[1024,128]{1,0:T(8,128)(2,1)} %k_hbm.1, bf16[1024,128]{1,0:T(8,128)(2,1)} %v_hbm.1, f32[6]{0:T(128)} %sink_ref.1, bf16[384,2048]{1,0:T(8,128)(2,1)} %proj_hbm.1, f32[1,2048]{1,0:T(1,128)} %bitcast.5, ...), custom_call_target="tpu_custom_call" | custom-call | tf_op jit(solution)/shard_map/pallas_call | solution.py:636
  117.4 2.3 %copy.14 = bf16[1024,512]{1,0:T(8,128)(2,1)} copy(bf16[1024,512]{1,0:T(8,128)(2,1)} %shard_map.118) | data formatting | bytes 2097152

commit v7 on v6

--- a/solution.py
+++ b/solution.py
@@ -10,11 +10,11 @@
 WINDOW = 128
 EPS = 1e-06
 MIX = 4
+PIECES = 4
 PROJECTION = (0, 1, 2, 3, 4)
 WEIGHTS = (2, 2, 4, 4, 4, 7, 8, 9, 11), (2, 2, 6, 4, 4, 8, 9, 10, 11)
 PREPARE, FEED, SECOND = (11, 12, 13, 14), (12, 13, 14, 15), (13, 14, 15, 16)
 SUM, FINISH = (14, 15, 16, 17), (15, 16, 17, 18)
-DRAIN = 9
 MESH = pl.DeviceIdType.MESH
 F32 = jnp.float32
 BF16 = jnp.bfloat16
@@ -43,12 +43,12 @@
         to = self.right if m % 2 == 0 else self.left
         return tp_copy(
             self.sent.at[slot, m], self.got.at[slot, m],
-            self.send.at[slot], self.recv.at[slot, 0 if m < 2 else 1], to,
+            self.send, self.recv.at[slot, 0 if m < 2 else 1], to,
         )
 
     def arrived(self, slot, group):
         ref = self.got.at[slot, pl.ds(2 * group, 2 + 2 * group)]
-        tp_copy(ref, ref, self.send.at[slot], self.recv.at[slot, group], self.right).wait_recv()
+        tp_copy(ref, ref, self.send, self.recv.at[slot, group], self.right).wait_recv()
 
     def first(self, slot, part):
         self.sent[slot, 0] = part(self.far, 0)
@@ -85,9 +85,8 @@
         )
         return half0, half1
 
-    def drain(self, slot):
-        ref = self.sent.at[slot]
-        tp_copy(ref, ref, self.send.at[slot], self.recv.at[slot, 0], self.right).wait_send()
+    def drain(self):
+        tp_copy(self.sent, self.sent, self.send, self.recv.at[0, 0], self.right).wait_send()
 
 
 class Squares:
@@ -99,12 +98,12 @@
         for m, to in enumerate((self.right, self.left, self.far)):
             yield tp_copy(
                 self.mine.at[slot], self.got.at[slot, m],
-                self.send.at[slot], self.recv.at[slot], to,
+                self.send, self.recv.at[slot], to,
             )
 
     def all(self, slot):
         ref = self.got.at[slot]
-        return tp_copy(ref, ref, self.send.at[slot], self.recv.at[slot], self.right)
+        return tp_copy(ref, ref, self.send, self.recv.at[slot], self.right)
 
     def give(self, slot, half0, half1):
         total = jnp.sum(half0 * half0, axis=1, keepdims=True) + jnp.sum(
@@ -125,8 +124,8 @@
         ]
         return columns[0] if len(columns) == 1 else jnp.concatenate(columns, axis=0)
 
-    def drain(self, slot):
-        self.all(slot).wait_send()
+    def drain(self):
+        tp_copy(self.got, self.got, self.send, self.recv.at[0], self.right).wait_send()
 
 
 class Gather:
@@ -136,11 +135,11 @@
 
     def copy(self, slot, owner, to, group, part):
         ref = self.buffer.at[owner, slot, part]
-        return tp_copy(ref, ref, self.send.at[slot], self.recv.at[slot, group], to)
+        return tp_copy(ref, ref, self.send, self.recv.at[slot, group], to)
 
     def some(self, slot, blocks, group):
         ref = self.buffer.at[pl.ds(0, blocks), slot]
-        return tp_copy(ref, ref, self.send.at[slot], self.recv.at[slot, group], self.right)
+        return tp_copy(ref, ref, self.send, self.recv.at[slot, group], self.right)
 
     def open(self, slot):
         whole = pl.ds(0, WINDOW)
@@ -155,8 +154,9 @@
     def close(self, slot):
         self.some(slot, 1, 1).wait_recv()
 
-    def drain(self, slot):
-        self.some(slot, 3, 0).wait_send()
+    def drain(self):
+        ref = self.buffer.at[pl.ds(0, 3)]
+        tp_copy(ref, ref, self.send, self.recv.at[0, 0], self.right).wait_send()
 
 
 class Projection:
@@ -292,7 +292,7 @@
         to = self.device(way, *((1 if m % 2 == 0 else 3, 0) if stage == 0 else (0, 1 if m % 2 == 0 else 3)), self.core)
         return pltpu.make_async_remote_copy(
             src_ref=ref, dst_ref=ref,
-            send_sem=self.send.at[way, stage], recv_sem=self.recv.at[way, stage, 0 if m < 2 else 1],
+            send_sem=self.send.at[way], recv_sem=self.recv.at[way, stage, 0 if m < 2 else 1],
             device_id={"sp": to}, device_id_type=MESH,
         )
 
@@ -300,7 +300,7 @@
         ref = self.rows(way, a, b, self.core)
         return pltpu.make_async_remote_copy(
             src_ref=ref, dst_ref=ref,
-            send_sem=self.core_send.at[way, a], recv_sem=self.core_recv.at[way, a],
+            send_sem=self.core_send.at[way], recv_sem=self.core_recv.at[way],
             device_id={"sp": self.device(way, 0, 0, 1 - self.core)}, device_id_type=MESH,
         )
 
@@ -316,7 +316,7 @@
         self.copy(way, stage, 1).start()
 
     def relay(self, way, stage):
-        self.some(64, self.send.at[way, stage], self.recv.at[way, stage, 0]).wait_recv()
+        self.some(64, self.send.at[way], self.recv.at[way, stage, 0]).wait_recv()
         self.copy(way, stage, 2).start()
         self.copy(way, stage, 3).start()
 
@@ -325,7 +325,7 @@
             self.over(way, *self.at(stage, k)).start()
 
     def close(self, way, stage):
-        self.some(32, self.send.at[way, stage], self.recv.at[way, stage, 1]).wait_recv()
+        self.some(32, self.send.at[way], self.recv.at[way, stage, 1]).wait_recv()
         self.share(way, stage, (2,))
 
     def step(self, way, n):
@@ -356,15 +356,12 @@
             for stage in (2, 3, 4):
                 self.close(way, stage)
         elif n == 8:
-            for a in range(4):
-                self.some(128, self.core_send.at[way, a], self.core_recv.at[way, a]).wait_recv()
+            self.some(512, self.core_send.at[way], self.core_recv.at[way]).wait_recv()
 
     def drain(self):
         for way in (0, 1):
-            for stage in range(5):
-                self.some(96, self.send.at[way, stage], self.recv.at[way, stage, 0]).wait_send()
-            for a in range(4):
-                self.some(128, self.core_send.at[way, a], self.core_recv.at[way, a]).wait_send()
+            self.some(480, self.send.at[way], self.recv.at[way, 0, 0]).wait_send()
+            self.some(512, self.core_send.at[way], self.core_recv.at[way]).wait_send()
 
 
 def layer_kernel(
@@ -372,7 +369,7 @@
     res_hbm, q_hbm, k_hbm, v_hbm, sink_ref, proj_hbm, gain_mix_ref, gain_pre_ref, gain_post_ref,
     gate_hbm, up_hbm, down_hbm,
     out_hbm,
-    done, res_ref, q_ref, k_ref, v_ref, proj_ref, gate_ref, up_ref, down_ref,
+    done, res_ref, q_ref, k_ref, v_ref, gate_ref, up_ref, down_ref,
     whole, keys, keys_turned, values, values_turned, taken, att,
     mixed, mine, squares, rows,
     normed, hidden, f_sent, f_got, f_own, f_total, f_mine, f_squares,
@@ -389,10 +386,11 @@
     units = gate_ref.shape[1]
     tiles = units // 128
     inner = 2 * units
+    projection = Projection(taken, proj_hbm, p_send, p_recv)
     loads = [
         pltpu.make_async_copy(a, b, load_sem.at[n])
         for n, (a, b) in enumerate((
-            (proj_hbm, proj_ref), (k_hbm, k_ref), (v_hbm, v_ref), (gate_hbm, gate_ref),
+            (proj_hbm.at[:, projection.columns(me)], taken.at[0]), (k_hbm, k_ref), (v_hbm, v_ref), (gate_hbm, gate_ref),
             (up_hbm, up_ref), (down_hbm, down_ref), (q_hbm, q_ref), (res_hbm, res_ref),
         ))
     ]
@@ -404,9 +402,10 @@
     others += [{"sp": n} for n in weights.neighbours()]
     for other in others:
         pl.semaphore_signal(barrier, inc=1, device_id=other, device_id_type=MESH)
-    for load in loads[:3]:
+    pl.semaphore_wait(barrier, len(others))
+    projection.step(0)
+    for load in loads[1:3]:
         load.wait()
-    pl.semaphore_wait(barrier, len(others))
 
     def halo(n):
         mine_ref, both = ((k_ref, keys), (v_ref, values))[n // 2]
@@ -419,8 +418,6 @@
             device_id={"sp": to}, device_id_type=MESH,
         )
 
-    projection = Projection(taken, proj_ref, p_send, p_recv)
-    projection.step(0)
     halos = keys.at[pl.ds(0, 4 * WINDOW)]
     halos = tp_copy(halos, halos, halo_send, halo_recv, right)
     for n in range(4):
@@ -444,9 +441,8 @@
     weights.open(0, 1)
     weights.over(0, 0, 0).start()
     weights.over(1, 0, 0).start()
-    for load in loads[6:]:
+    for load in loads[6:] + loads[:1]:
         load.wait()
-    taken[0] = proj_ref[:, projection.columns(me)]
 
     mixing = Gather(att, at_send, at_recv)
     feeding = Gather(rows, ag_send, ag_recv)
@@ -541,15 +537,6 @@
         at = pl.ds(place(slot), WINDOW)
         return pltpu.make_async_copy(done.at[at, :], out_hbm.at[at, :], out_sem)
 
-    def drain(slot):
-        mixing.drain(slot)
-        sums.drain(slot)
-        feeding.drain(slot)
-
-    def f_drain(u):
-        f_scatter.drain(u)
-        f_sums.drain(u)
-
     def step(t, carry):
         def when(lag, fn):
             @pl.when((t >= lag) & (t < chunks + lag))
@@ -595,20 +582,36 @@
         when_fed(SECOND, f_scatter.second)
         when_fed(SUM, feed_sum)
         when_fed(FINISH, finish)
-        when(DRAIN, drain)
-
-        @pl.when(t == SECOND[0])
+        @pl.when(t == FEED[3])
         def _():
             halos.wait_send()
             weights.drain()
             projection.drain()
-
-        when_fed(FINISH[1:], f_drain)
+            mixing.drain()
+            feeding.drain()
+            sums.drain()
+
         return carry
 
     lax.fori_loop(0, FINISH[-1] + 1, step, 0)
-    f_drain(half_chunks - 1)
+    f_scatter.drain()
+    f_sums.drain()
     pltpu.make_async_copy(done, out_hbm, out_sem).wait()
+
+
+def pass_kernel(in_hbm, out_hbm, held, in_sem, out_sem):
+    size = held.shape[0] // PIECES
+    ins, outs = [], []
+    for n in range(PIECES):
+        at = pl.ds(n * size, size)
+        ins.append(pltpu.make_async_copy(in_hbm.at[at, :], held.at[at, :], in_sem.at[n]))
+        outs.append(pltpu.make_async_copy(held.at[at, :], out_hbm.at[at, :], out_sem))
+    for copy in ins:
+        copy.start()
+    for copy, out in zip(ins, outs):
+        copy.wait()
+        out.start()
+    pltpu.make_async_copy(held, out_hbm, out_sem).wait()
 
 
 def sems(*shapes):
@@ -633,13 +636,13 @@
         residual, rotated_query_rows, rotated_key_rows, value_matrix_rows, out_proj,
         gate_proj, up_proj, down_proj.T,
     )
-    return pl.pallas_call(
+    result = pl.pallas_call(
         functools.partial(layer_kernel, chunks, sp_count),
         out_shape=jax.ShapeDtypeStruct(residual.shape, BF16),
         in_specs=[hbm] * 4 + [smem, hbm] + [vmem] * 3 + [hbm] * 3,
         out_specs=hbm,
         scratch_shapes=[pltpu.VMEM(residual.shape, BF16)]
-        + [pltpu.VMEM(a.shape, BF16) for a in loaded]
+        + [pltpu.VMEM(a.shape, BF16) for a in loaded[:4] + loaded[5:]]
         + [pltpu.VMEM((full, 3 * units), BF16)]
         + [pltpu.VMEM((length + big, 128), BF16)] * 4
         + [
@@ -659,10 +662,8 @@
             pltpu.VMEM((half, 3, 16, 128), F32),
         ]
         + [pltpu.SemaphoreType.DMA]
-        + sems((8,), (2, 5), (2, 5, 2), (2, 4), (2, 4))
-        + [pltpu.SemaphoreType.DMA] * 2
-        + sems((3,), (4,), (chunks,), (chunks, 2), (chunks,), (chunks,), (chunks,), (chunks, 2))
-        + sems((half,), (half, 2), (half,), (half,)),
+        + sems((8,), (2,), (2, 5, 2), (2,), (2,), (), (), (3,), (4,), (), (chunks, 2), (), (chunks,))
+        + sems((), (chunks, 2), (), (half, 2), (), (half,)),
         compiler_params=pltpu.CompilerParams(
             collective_id=0, has_side_effects=True, vmem_limit_bytes=54 * 2**20
         ),
@@ -670,6 +671,13 @@
         residual, rotated_query_rows, rotated_key_rows, value_matrix_rows, head_sink_logit,
         out_proj, gain_mix[None], gain_pre[None], gain_post[None], *loaded[5:],
     )
+    return pl.pallas_call(
+        pass_kernel,
+        out_shape=jax.ShapeDtypeStruct(residual.shape, BF16),
+        in_specs=[hbm],
+        out_specs=hbm,
+        scratch_shapes=[pltpu.VMEM(residual.shape, BF16)] + sems((PIECES,), ()),
+    )(result)
 
 
 def solution(mesh):

time: 120 us -> 119 us (level)
  local copies, waits for them, and re-layouts: 2.26 us -> 0 us
  Pallas kernels: 117 us -> 119 us
    unnamed x1 -> x0, local copies, waits for them, and re-layouts: 2.26 us -> none
    pallas_call x0 -> x1, Pallas kernels: none -> 1.95 us  [body(): pl.pallas_call(pass_kernel, out_shape=jax.ShapeDtypeStruct(residual.shape...]
where the time goes in v7:
time: 119 us
  Pallas kernels  119 us (100%)
    pallas_call x1, Pallas kernels, body(): pl.pallas_call(functools.partial(layer_kernel, chunks, sp_count), out_sha...  117 us

profile of v7, /device:TPU:0, one launch (start us, length us, event | category | flops | bytes accessed | tf_op | source)
XLA Modules:
  0.0 118.8 jit_solution(5427094222603616312)
XLA Ops:
  0.0 116.8 %shard_map.118.in_hbm = bf16[1024,512]{1,0:T(8,128)(2,1)} custom-call(bf16[1024,512]{1,0:T(8,128)(2,1)} %res_hbm.1, bf16[1024,384]{1,0:T(8,128)(2,1)} %q_hbm.1, bf16[1024,128]{1,0:T(8,128)(2,1)} %k_hbm.1, bf16[1024,128]{1,0:T(8,128)(2,1)} %v_hbm.1, f32[6]{0:T(128)} %sink_ref.1, bf16[384,2048]{1,0:T(8,128)(2,1)} %proj_hbm.1, f32[1,2048]{1,0:T(1,128)} %bitcast.5, ...), custom_call_target="tpu_custom_call" | custom-call | tf_op jit(solution)/shard_map/pallas_call | solution.py:639
  116.8 2.0 %shard_map.119 = bf16[1024,512]{1,0:T(8,128)(2,1)} custom-call(bf16[1024,512]{1,0:T(8,128)(2,1)} %shard_map.118.in_hbm), custom_call_target="tpu_custom_call" | custom-call | tf_op jit(solution)/shard_map/pallas_call | solution.py:674

commit v8 on v7

--- a/solution.py
+++ b/solution.py
@@ -578,8 +578,8 @@
             prepare(3)
 
 
+        when_fed(SECOND, f_scatter.second)
         when_fed(FEED, feed)
-        when_fed(SECOND, f_scatter.second)
         when_fed(SUM, feed_sum)
         when_fed(FINISH, finish)
         @pl.when(t == FEED[3])

time: 119 us -> 119 us (level)
  no operation moved by 1% of the time
where the time goes in v8:
time: 119 us
  Pallas kernels  119 us (100%)
    pallas_call x1, Pallas kernels, body(): pl.pallas_call(functools.partial(layer_kernel, chunks, sp_count), out_sha...  117 us

profile of v8, /device:TPU:0, one launch (start us, length us, event | category | flops | bytes accessed | tf_op | source)
XLA Modules:
  0.0 118.9 jit_solution(4122233940106744015)
XLA Ops:
  0.0 116.9 %shard_map.118.in_hbm = bf16[1024,512]{1,0:T(8,128)(2,1)} custom-call(bf16[1024,512]{1,0:T(8,128)(2,1)} %res_hbm.1, bf16[1024,384]{1,0:T(8,128)(2,1)} %q_hbm.1, bf16[1024,128]{1,0:T(8,128)(2,1)} %k_hbm.1, bf16[1024,128]{1,0:T(8,128)(2,1)} %v_hbm.1, f32[6]{0:T(128)} %sink_ref.1, bf16[384,2048]{1,0:T(8,128)(2,1)} %proj_hbm.1, f32[1,2048]{1,0:T(1,128)} %bitcast.5, ...), custom_call_target="tpu_custom_call" | custom-call | tf_op jit(solution)/shard_map/pallas_call | solution.py:639
  116.9 2.0 %shard_map.119 = bf16[1024,512]{1,0:T(8,128)(2,1)} custom-call(bf16[1024,512]{1,0:T(8,128)(2,1)} %shard_map.118.in_hbm), custom_call_target="tpu_custom_call" | custom-call | tf_op jit(solution)/shard_map/pallas_call | solution.py:674
